TPU v7x, 512 devices: a whole 4x4x16 slice. The times are simulated.
512 devices in a mesh: sp: 128 (over z, x, core), tp: 4 (over y).
Axes of the slice: x: 4, y: 4, z: 16, core: 2. Of those that a mesh axis runs over, the one named last changes fastest.
Arguments:
- stream: bfloat16 [16384, 2048], P('sp', 'tp'), may hold values from -6 to 6
- norm_gain: float32 [2048], replicated, may hold values from 0.1 to 1.9
- w_query: bfloat16 [2048, 1024], P('sp', 'tp'), may hold values from -0.75 to 0.75
- w_key: bfloat16 [2048, 256], P('sp', 'tp'), may hold values from -0.125 to 0.125
- w_value: bfloat16 [2048, 256], P('sp', 'tp'), may hold values from -0.125 to 0.125
- w_conv_in: bfloat16 [2048, 1024], P('sp', 'tp'), may hold values from -0.125 to 0.125
- w_conv_gate: bfloat16 [2048, 1024], P('sp', 'tp'), may hold values from -0.125 to 0.125
- conv_taps: float32 [3, 1024], P(None, 'tp'), may hold values from -3.5 to 3.5
- sb_bias: float32 [16], P('tp'), may hold values from -28 to -13
- w_out_attn: bfloat16 [1024, 2048], P('tp', 'sp'), may hold values from -0.5 to 0.5
- w_out_conv: bfloat16 [1024, 2048], P('tp', 'sp'), may hold values from -0.125 to 0.125
Outputs:
- mixed: bfloat16 [16384, 2048], P('sp', 'tp')
- log_weight_sum: float32 [16, 16384], P('tp', 'sp')
All inputs are finite; a program needn't handle non-finite values.
Results may differ from a plain program's by a relative error of at most 0.013.
The roundings to bfloat16 on the way count: a program that leaves them out, or rounds other values in their place, can miss the bound.
Values may be sent and summed in bfloat16 or wider, within the bound.
A program may use at most 64 MiB of HBM per device.

v0:
```python
import jax
import jax.numpy as jnp
from jax import lax
from jax.sharding import Mesh
from jax.sharding import PartitionSpec as P

D = 2048
HEAD = 64
CONV_K = 3
SP = ("sp_0", "sp_1", "sp_2")


EPS = 1e-06
FLOOR = 0.02


def side_by_side(arrays, axis, dim, along):
    ends, at = ([], 0)
    for a in arrays[:-1]:
        at += a.shape[along]
        ends.append(at)
    both = jnp.concatenate(arrays, axis=along)
    return tuple(jnp.split(lax.all_gather(both, axis, axis=dim, tiled=True), ends, axis=along))


def copy_for_each(value, axis):
    copies = jnp.broadcast_to(value, (lax.axis_size(axis), *value.shape))
    return lax.all_to_all(copies, axis, split_axis=0, concat_axis=0, tiled=True)


def in_order(parts, dim):
    dims = list(parts.shape[1:])
    dims[dim] *= parts.shape[0]
    return jnp.moveaxis(parts, 0, dim).reshape(dims)


def collect(value, axis, dim):
    parts = copy_for_each(value, axis)
    return in_order(parts, dim)


def from_behind(value, axis, steps):
    count = lax.axis_size(axis)
    leading, last = (max(0, -steps), min(count, count - steps))
    return lax.ppermute(value, axis, [(source, source + steps) for source in range(leading, last)])


def gather_in_order(value, axes, order):
    parts = value
    for k in order:
        parts = lax.all_gather(parts, axes[k])
    done = order[::-1]
    back = [done.index(k) for k in range(len(axes))]
    parts = parts.transpose(*back, *range(len(axes), parts.ndim))
    return parts.reshape(-1, *value.shape)


def gather_axes(value, axes, order, dim):
    return in_order(gather_in_order(value, axes, order), dim)


def split_up(value, dim, size):
    dims = value.shape
    parts = value.reshape(*dims[:dim], size, dims[dim] // size, *dims[dim + 1 :])
    return jnp.moveaxis(parts, dim, 0)


def summed_on_arrival(value, axis, dim):
    size = lax.axis_size(axis)
    parts = lax.all_to_all(split_up(value, dim, size), axis, 0, 0, tiled=True)
    return jnp.sum(parts.astype(jnp.float32), axis=0)


def head_scores(query_head, key_rows, key_pos, query_pos, offset):
    scores = (
        jnp.einsum("qd,kd->qk", query_head, key_rows, preferred_element_type=jnp.float32)
        * HEAD ** (-0.5)
        + offset
    )
    causal = key_pos[None, :] < query_pos[:, None]
    fails = jnp.where(causal, jax.nn.log_sigmoid(-scores), 0.0)
    return (scores, causal, fails)


def split_heads(query):
    return [query[:, head * HEAD : (head + 1) * HEAD] for head in range(query.shape[1] // HEAD)]


def sweep_keys(all_keys, all_values, query, first, tokens, sb_bias):
    rows = query.shape[0]
    query_heads = split_heads(query)
    heads = len(query_heads)
    query_pos = first + jnp.arange(rows, dtype=jnp.int32)
    span = 8 * tokens
    spans = all_keys.shape[0] // span
    my_span = first // span

    def turn(step, carry):

        def work(state):
            outs, survs = state
            begin = (my_span - step) * span
            key_rows = lax.dynamic_slice_in_dim(all_keys, begin, span, 0)
            value_rows = lax.dynamic_slice_in_dim(all_values, begin, span, 0)
            key_pos = begin + jnp.arange(span, dtype=jnp.int32)
            added_outs = []
            added_survs = []
            for head in range(heads):
                scores, causal, fails = head_scores(
                    query_heads[head], key_rows, key_pos, query_pos, sb_bias[head]
                )
                later = lax.cumsum(fails, axis=1, reverse=True) - fails + survs[head][:, None]
                stick = jnp.where(causal, jnp.exp(jax.nn.log_sigmoid(scores) + later), 0.0).astype(
                    jnp.bfloat16
                )
                added_outs.append(
                    outs[head] + jnp.dot(stick, value_rows, preferred_element_type=jnp.float32)
                )
                added_survs.append(survs[head] + jnp.sum(fails, axis=1))
            return (jnp.stack(added_outs), jnp.stack(added_survs))

        return lax.cond(step <= my_span, work, lambda state: state, carry)

    start_state = (
        jnp.zeros((heads, rows, HEAD), jnp.float32),
        jnp.zeros((heads, rows), jnp.float32),
    )
    return lax.fori_loop(0, spans, turn, start_state)


def local(
    stream,
    norm_gain,
    w_query,
    w_key,
    w_value,
    w_conv_in,
    w_conv_gate,
    conv_taps,
    sb_bias,
    w_out_attn,
    w_out_conv,
):
    tokens = stream.shape[0]
    weights = side_by_side((w_query, w_key, w_value, w_conv_in, w_conv_gate), SP, 0, 1)
    piece_f = collect(stream, "tp", 1).astype(jnp.float32)
    scaled = (piece_f * norm_gain[None, :]).astype(jnp.bfloat16)
    sums = tuple(
        (jnp.dot(scaled, weight, preferred_element_type=jnp.float32) for weight in weights)
    )
    sums, squares = (sums, jnp.sum(piece_f * piece_f, axis=1))
    row_scale = lax.rsqrt(squares / D + EPS)[:, None]
    query, keys, values, conv_in, conv_gate = [
        (total * row_scale).astype(jnp.bfloat16) for total in sums
    ]
    previous = from_behind(conv_in[tokens - (CONV_K - 1) :], SP, 1)
    padded = jnp.concatenate([previous, conv_in], axis=0).astype(jnp.float32)
    conv_mixed = jnp.zeros((tokens, conv_in.shape[1]), jnp.float32)
    for tap in range(CONV_K):
        conv_mixed = conv_mixed + conv_taps[tap][None, :] * padded[tap : tap + tokens]
    conv_out = (conv_gate.astype(jnp.float32) * conv_mixed).astype(jnp.bfloat16)
    heads = query.shape[1] // HEAD
    my_index = lax.axis_index(SP)
    groups = [(query, my_index * tokens)]
    all_keys, all_values = side_by_side((keys, values), SP, 0, 1)
    results = [
        sweep_keys(all_keys, all_values, rows_in, first, tokens, sb_bias)
        for rows_in, first in groups
    ]
    attended = results[0][0].astype(jnp.bfloat16)
    survs = results[0][1]
    log_weight_sum = jnp.log(jnp.maximum(-jnp.expm1(survs), FLOOR))
    attended_weight, conv_weight = (
        gather_axes(w_out_attn, SP, (1, 0, 2), 1),
        gather_axes(w_out_conv, SP, (1, 0, 2), 1),
    )
    partial_value = jnp.einsum(
        "hqd,hde->qe",
        attended,
        attended_weight.reshape(heads, HEAD, attended_weight.shape[1]),
        preferred_element_type=jnp.float32,
    )
    partial_value = partial_value + jnp.dot(
        conv_out, conv_weight, preferred_element_type=jnp.float32
    )
    mixed = summed_on_arrival(partial_value.astype(jnp.bfloat16), "tp", 1).astype(jnp.bfloat16)
    return (mixed, log_weight_sum)


def solution(mesh):
    torus = Mesh(mesh.devices.reshape(16, 4, 2, mesh.shape["tp"]), ("sp_0", "sp_1", "sp_2", "tp"))
    return jax.shard_map(
        local,
        mesh=torus,
        in_specs=(
            P(SP, "tp"),
            P(),
            P(SP, "tp"),
            P(SP, "tp"),
            P(SP, "tp"),
            P(SP, "tp"),
            P(SP, "tp"),
            P(None, "tp"),
            P("tp"),
            P("tp", SP),
            P("tp", SP),
        ),
        out_specs=(P(SP, "tp"), P("tp", SP)),
        check_vma=False,
    )
```

profile of v0, /device:TPU:480, one launch (start us, length us, event | category | flops | bytes accessed | tf_op | source)
XLA Modules:
  0.0 752.4 jit_solution(10551346437414015456)
XLA Ops:
  8.7 12.5 %all-gather = bf16[1024,16]{0,1:T(8,128)(2,1)S(1)} all-gather(bf16[256,16]{0,1:T(8,128)(2,1)} %param.24), channel_id=2, replica_groups=mesh['sp_0'=16,'sp_1'=4,'sp_2'=2,'tp'=4] {'sp_1'}, dimensions={0}, use_global_device_ids=true | all-gather | bytes 40960 | tf_op jit(solution)/shard_map/all_gather | solution.py:51
  21.2 31.2 %all-gather.1 = bf16[64,256,16]{1,2,0:T(8,128)(2,1)} all-gather(bf16[4,256,16]{1,2,0:T(8,128)(2,1)S(1)} %bitcast.149), channel_id=3, replica_groups=mesh['sp_0'=16,'sp_1'=4,'sp_2'=2,'tp'=4] {'sp_0'}, dimensions={0}, use_global_device_ids=true | all-gather | bytes 557056 | tf_op jit(solution)/shard_map/all_gather | solution.py:51
  54.4 4.5 all-to-all-start
  59.0 12.1 %all-gather.3 = bf16[1024,16]{0,1:T(8,128)(2,1)S(1)} all-gather(bf16[256,16]{0,1:T(8,128)(2,1)} %param.25), channel_id=5, replica_groups=mesh['sp_0'=16,'sp_1'=4,'sp_2'=2,'tp'=4] {'sp_1'}, dimensions={0}, use_global_device_ids=true | all-gather | bytes 40960 | tf_op jit(solution)/shard_map/all_gather | solution.py:51
  71.1 33.5 %all-gather.4 = bf16[64,256,16]{1,2,0:T(8,128)(2,1)} all-gather(bf16[4,256,16]{1,2,0:T(8,128)(2,1)S(1)} %bitcast.150), channel_id=6, replica_groups=mesh['sp_0'=16,'sp_1'=4,'sp_2'=2,'tp'=4] {'sp_0'}, dimensions={0}, use_global_device_ids=true | all-gather | bytes 557056 | tf_op jit(solution)/shard_map/all_gather | solution.py:51
  105.3 44.9 %all-gather.11.cloned.1.call-done = bf16[2048,896]{1,0:T(8,128)(2,1)} async-done(((bf16[16,896]{1,0:T(8,128)(2,1)}), bf16[2048,896]{1,0:T(8,128)(2,1)}) %all-gather.11.cloned.1.call-update) | async-done | bytes 3670032 | tf_op jit(solution)/shard_map/all_gather | solution.py:23
  154.5 15.4 %all-gather.15.cloned.1.call-done = bf16[32,4,256,16]{2,3,1,0:T(8,128)(2,1)} async-done(((bf16[16,4,256,16]{2,3,1,0:T(8,128)(2,1)}), bf16[32,4,256,16]{2,3,1,0:T(8,128)(2,1)}) %all-gather.15.cloned.1.call-update) | async-done | bytes 1048592 | tf_op jit(solution)/shard_map/all_gather | solution.py:51
  173.1 19.8 %all-gather.17.cloned.1.call-done = bf16[32,4,256,16]{2,3,1,0:T(8,128)(2,1)} async-done(((bf16[16,4,256,16]{2,3,1,0:T(8,128)(2,1)}), bf16[32,4,256,16]{2,3,1,0:T(8,128)(2,1)}) %all-gather.17.cloned.1.call-update) | async-done | bytes 1048592 | tf_op jit(solution)/shard_map/all_gather | solution.py:51
  204.5 128.5 %all-gather.13.cloned.1.call-done = bf16[16384,128]{0,1:T(8,128)(2,1)} async-done(((bf16[128,128]{0,1:T(8,128)(2,1)}), bf16[16384,128]{0,1:T(8,128)(2,1)}) %all-gather.13.cloned.1.call-update) | async-done | bytes 4194320 | tf_op jit(solution)/shard_map/all_gather | solution.py:23
  336.9 4.8 copy.76
  344.8 380.3 %while.16 = (s32[]{:T(128)}, f32[4,128,64]{1,2,0:T(8,128)S(1)}, f32[4,128]{1,0:T(4,128)S(1)}, s32[]{:T(128)}, bf16[16384,64]{1,0:T(8,128)(2,1)}, /*index=5*/bf16...) while((s32[]{:T(128)}, f32[4,128,64]{1,2,0:T(8,128)S(1)}, ...), condition=%wide.region_16.17_spmd.clone, body=%wide.region_1.16_spmd.clone.sunk | while | flops 218663040 | bytes 27026348 | solution.py:128
  345.1 23.7 %conditional.3 = ((f32[4,128,64]{1,2,0:T(8,128)S(1)}, f32[4,128]{1,0:T(4,128)S(1)})) conditional(s32[]{:T(128)} %convert_element_type.120, (f32[4,128,64]{1,2,0:T(8,128)S(1)}, f32[4,128]{1,0:T(4,128)S(1)}) %tuple.77, (f32[4,128,64]{1,2,0:T(8,128)S(1)}, s32[]{:T(128)}, s32[]{:T(128)}, s32[]{:T(128)}, bf16[16384,64]{1,0:T(8,128)(2,1)}, ...), branch_computations={%region_2.2_spmd, %region_3.15_spmd} | conditional | flops 218663040 | bytes 27025578 | solution.py:122
  357.2 4.5 fusion.62
  368.8 23.7 %conditional.3 = ((f32[4,128,64]{1,2,0:T(8,128)S(1)}, f32[4,128]{1,0:T(4,128)S(1)})) conditional(s32[]{:T(128)} %convert_element_type.120, (f32[4,128,64]{1,2,0:T(8,128)S(1)}, f32[4,128]{1,0:T(4,128)S(1)}) %tuple.77, (f32[4,128,64]{1,2,0:T(8,128)S(1)}, s32[]{:T(128)}, s32[]{:T(128)}, s32[]{:T(128)}, bf16[16384,64]{1,0:T(8,128)(2,1)}, ...), branch_computations={%region_2.2_spmd, %region_3.15_spmd} | conditional | flops 218663040 | bytes 27025578 | solution.py:122
  381.0 4.5 fusion.62
  392.6 23.7 %conditional.3 = ((f32[4,128,64]{1,2,0:T(8,128)S(1)}, f32[4,128]{1,0:T(4,128)S(1)})) conditional(s32[]{:T(128)} %convert_element_type.120, (f32[4,128,64]{1,2,0:T(8,128)S(1)}, f32[4,128]{1,0:T(4,128)S(1)}) %tuple.77, (f32[4,128,64]{1,2,0:T(8,128)S(1)}, s32[]{:T(128)}, s32[]{:T(128)}, s32[]{:T(128)}, bf16[16384,64]{1,0:T(8,128)(2,1)}, ...), branch_computations={%region_2.2_spmd, %region_3.15_spmd} | conditional | flops 218663040 | bytes 27025578 | solution.py:122
  404.7 4.5 fusion.62
  416.3 23.7 %conditional.3 = ((f32[4,128,64]{1,2,0:T(8,128)S(1)}, f32[4,128]{1,0:T(4,128)S(1)})) conditional(s32[]{:T(128)} %convert_element_type.120, (f32[4,128,64]{1,2,0:T(8,128)S(1)}, f32[4,128]{1,0:T(4,128)S(1)}) %tuple.77, (f32[4,128,64]{1,2,0:T(8,128)S(1)}, s32[]{:T(128)}, s32[]{:T(128)}, s32[]{:T(128)}, bf16[16384,64]{1,0:T(8,128)(2,1)}, ...), branch_computations={%region_2.2_spmd, %region_3.15_spmd} | conditional | flops 218663040 | bytes 27025578 | solution.py:122
  428.5 4.5 fusion.62
  440.1 23.7 %conditional.3 = ((f32[4,128,64]{1,2,0:T(8,128)S(1)}, f32[4,128]{1,0:T(4,128)S(1)})) conditional(s32[]{:T(128)} %convert_element_type.120, (f32[4,128,64]{1,2,0:T(8,128)S(1)}, f32[4,128]{1,0:T(4,128)S(1)}) %tuple.77, (f32[4,128,64]{1,2,0:T(8,128)S(1)}, s32[]{:T(128)}, s32[]{:T(128)}, s32[]{:T(128)}, bf16[16384,64]{1,0:T(8,128)(2,1)}, ...), branch_computations={%region_2.2_spmd, %region_3.15_spmd} | conditional | flops 218663040 | bytes 27025578 | solution.py:122
  463.8 23.7 %conditional.3 = ((f32[4,128,64]{1,2,0:T(8,128)S(1)}, f32[4,128]{1,0:T(4,128)S(1)})) conditional(s32[]{:T(128)} %convert_element_type.120, (f32[4,128,64]{1,2,0:T(8,128)S(1)}, f32[4,128]{1,0:T(4,128)S(1)}) %tuple.77, (f32[4,128,64]{1,2,0:T(8,128)S(1)}, s32[]{:T(128)}, s32[]{:T(128)}, s32[]{:T(128)}, bf16[16384,64]{1,0:T(8,128)(2,1)}, ...), branch_computations={%region_2.2_spmd, %region_3.15_spmd} | conditional | flops 218663040 | bytes 27025578 | solution.py:122
  487.6 23.7 %conditional.3 = ((f32[4,128,64]{1,2,0:T(8,128)S(1)}, f32[4,128]{1,0:T(4,128)S(1)})) conditional(s32[]{:T(128)} %convert_element_type.120, (f32[4,128,64]{1,2,0:T(8,128)S(1)}, f32[4,128]{1,0:T(4,128)S(1)}) %tuple.77, (f32[4,128,64]{1,2,0:T(8,128)S(1)}, s32[]{:T(128)}, s32[]{:T(128)}, s32[]{:T(128)}, bf16[16384,64]{1,0:T(8,128)(2,1)}, ...), branch_computations={%region_2.2_spmd, %region_3.15_spmd} | conditional | flops 218663040 | bytes 27025578 | solution.py:122
  511.3 23.7 %conditional.3 = ((f32[4,128,64]{1,2,0:T(8,128)S(1)}, f32[4,128]{1,0:T(4,128)S(1)})) conditional(s32[]{:T(128)} %convert_element_type.120, (f32[4,128,64]{1,2,0:T(8,128)S(1)}, f32[4,128]{1,0:T(4,128)S(1)}) %tuple.77, (f32[4,128,64]{1,2,0:T(8,128)S(1)}, s32[]{:T(128)}, s32[]{:T(128)}, s32[]{:T(128)}, bf16[16384,64]{1,0:T(8,128)(2,1)}, ...), branch_computations={%region_2.2_spmd, %region_3.15_spmd} | conditional | flops 218663040 | bytes 27025578 | solution.py:122
  535.1 23.7 %conditional.3 = ((f32[4,128,64]{1,2,0:T(8,128)S(1)}, f32[4,128]{1,0:T(4,128)S(1)})) conditional(s32[]{:T(128)} %convert_element_type.120, (f32[4,128,64]{1,2,0:T(8,128)S(1)}, f32[4,128]{1,0:T(4,128)S(1)}) %tuple.77, (f32[4,128,64]{1,2,0:T(8,128)S(1)}, s32[]{:T(128)}, s32[]{:T(128)}, s32[]{:T(128)}, bf16[16384,64]{1,0:T(8,128)(2,1)}, ...), branch_computations={%region_2.2_spmd, %region_3.15_spmd} | conditional | flops 218663040 | bytes 27025578 | solution.py:122
  558.9 23.7 %conditional.3 = ((f32[4,128,64]{1,2,0:T(8,128)S(1)}, f32[4,128]{1,0:T(4,128)S(1)})) conditional(s32[]{:T(128)} %convert_element_type.120, (f32[4,128,64]{1,2,0:T(8,128)S(1)}, f32[4,128]{1,0:T(4,128)S(1)}) %tuple.77, (f32[4,128,64]{1,2,0:T(8,128)S(1)}, s32[]{:T(128)}, s32[]{:T(128)}, s32[]{:T(128)}, bf16[16384,64]{1,0:T(8,128)(2,1)}, ...), branch_computations={%region_2.2_spmd, %region_3.15_spmd} | conditional | flops 218663040 | bytes 27025578 | solution.py:122
  582.6 23.7 %conditional.3 = ((f32[4,128,64]{1,2,0:T(8,128)S(1)}, f32[4,128]{1,0:T(4,128)S(1)})) conditional(s32[]{:T(128)} %convert_element_type.120, (f32[4,128,64]{1,2,0:T(8,128)S(1)}, f32[4,128]{1,0:T(4,128)S(1)}) %tuple.77, (f32[4,128,64]{1,2,0:T(8,128)S(1)}, s32[]{:T(128)}, s32[]{:T(128)}, s32[]{:T(128)}, bf16[16384,64]{1,0:T(8,128)(2,1)}, ...), branch_computations={%region_2.2_spmd, %region_3.15_spmd} | conditional | flops 218663040 | bytes 27025578 | solution.py:122
  606.4 23.7 %conditional.3 = ((f32[4,128,64]{1,2,0:T(8,128)S(1)}, f32[4,128]{1,0:T(4,128)S(1)})) conditional(s32[]{:T(128)} %convert_element_type.120, (f32[4,128,64]{1,2,0:T(8,128)S(1)}, f32[4,128]{1,0:T(4,128)S(1)}) %tuple.77, (f32[4,128,64]{1,2,0:T(8,128)S(1)}, s32[]{:T(128)}, s32[]{:T(128)}, s32[]{:T(128)}, bf16[16384,64]{1,0:T(8,128)(2,1)}, ...), branch_computations={%region_2.2_spmd, %region_3.15_spmd} | conditional | flops 218663040 | bytes 27025578 | solution.py:122
  630.1 23.7 %conditional.3 = ((f32[4,128,64]{1,2,0:T(8,128)S(1)}, f32[4,128]{1,0:T(4,128)S(1)})) conditional(s32[]{:T(128)} %convert_element_type.120, (f32[4,128,64]{1,2,0:T(8,128)S(1)}, f32[4,128]{1,0:T(4,128)S(1)}) %tuple.77, (f32[4,128,64]{1,2,0:T(8,128)S(1)}, s32[]{:T(128)}, s32[]{:T(128)}, s32[]{:T(128)}, bf16[16384,64]{1,0:T(8,128)(2,1)}, ...), branch_computations={%region_2.2_spmd, %region_3.15_spmd} | conditional | flops 218663040 | bytes 27025578 | solution.py:122
  653.9 23.7 %conditional.3 = ((f32[4,128,64]{1,2,0:T(8,128)S(1)}, f32[4,128]{1,0:T(4,128)S(1)})) conditional(s32[]{:T(128)} %convert_element_type.120, (f32[4,128,64]{1,2,0:T(8,128)S(1)}, f32[4,128]{1,0:T(4,128)S(1)}) %tuple.77, (f32[4,128,64]{1,2,0:T(8,128)S(1)}, s32[]{:T(128)}, s32[]{:T(128)}, s32[]{:T(128)}, bf16[16384,64]{1,0:T(8,128)(2,1)}, ...), branch_computations={%region_2.2_spmd, %region_3.15_spmd} | conditional | flops 218663040 | bytes 27025578 | solution.py:122
  677.6 23.7 %conditional.3 = ((f32[4,128,64]{1,2,0:T(8,128)S(1)}, f32[4,128]{1,0:T(4,128)S(1)})) conditional(s32[]{:T(128)} %convert_element_type.120, (f32[4,128,64]{1,2,0:T(8,128)S(1)}, f32[4,128]{1,0:T(4,128)S(1)}) %tuple.77, (f32[4,128,64]{1,2,0:T(8,128)S(1)}, s32[]{:T(128)}, s32[]{:T(128)}, s32[]{:T(128)}, bf16[16384,64]{1,0:T(8,128)(2,1)}, ...), branch_computations={%region_2.2_spmd, %region_3.15_spmd} | conditional | flops 218663040 | bytes 27025578 | solution.py:122
  701.4 23.7 %conditional.3 = ((f32[4,128,64]{1,2,0:T(8,128)S(1)}, f32[4,128]{1,0:T(4,128)S(1)})) conditional(s32[]{:T(128)} %convert_element_type.120, (f32[4,128,64]{1,2,0:T(8,128)S(1)}, f32[4,128]{1,0:T(4,128)S(1)}) %tuple.77, (f32[4,128,64]{1,2,0:T(8,128)S(1)}, s32[]{:T(128)}, s32[]{:T(128)}, s32[]{:T(128)}, bf16[16384,64]{1,0:T(8,128)(2,1)}, ...), branch_computations={%region_2.2_spmd, %region_3.15_spmd} | conditional | flops 218663040 | bytes 27025578 | solution.py:122
  735.8 9.3 %all-to-all-done.1 = bf16[4,128,512]{2,1,0:T(8,128)(2,1)S(1)} async-done(((bf16[4,128,512]{2,1,0:T(8,128)(2,1)}), bf16[4,128,512]{2,1,0:T(8,128)(2,1)S(1)}, u32[]{:S(2)}, u32[]{:S(2)}) %all-to-all-start.1) | async-done | bytes 524320 | tf_op jit(solution)/shard_map/all_to_all | solution.py:70
  (705 shorter events, 399.3 us)
Async XLA Ops:
  7.2 97.8 %copy-start.3 = (f32[2048]{0:T(1024)S(1)}, f32[2048]{0:T(1024)}, u32[]{:S(2)}) copy-start(f32[2048]{0:T(1024)} %param.16) | copy-start | bytes 24580
  7.2 143.1 %all-gather.11.cloned.1.call-start = ((), (), s32[]{:S(2)}) async-start(), calls=%async_computation.2 | async-start | bytes 3698688 | tf_op jit(solution)/shard_map/all_gather | solution.py:23
  8.7 161.2 %all-gather.15.cloned.1.call-start = ((), (), s32[]{:S(2)}) async-start(), calls=%async_computation.4 | async-start | bytes 1572864 | tf_op jit(solution)/shard_map/all_gather | solution.py:51
  52.5 101.4 %copy-start.4 = (f32[3,256]{1,0:T(4,128)S(1)}, f32[3,256]{1,0:T(4,128)}, u32[]{:S(2)}) copy-start(f32[3,256]{1,0:T(4,128)} %param.22) | copy-start | bytes 9220
  54.4 50.3 %all-to-all-start = ((bf16[4,128,512]{1,2,0:T(8,128)(2,1)}), bf16[4,128,512]{1,2,0:T(8,128)(2,1)S(1)}, u32[]{:S(2)}, u32[]{:S(2)}) async-start(bf16[4,128,512]{1,2,0:T(8,128)(2,1)} %broadcast_in_dim.30), calls=%async_computation | async-start | bytes 1048576 | tf_op jit(solution)/shard_map/all_to_all | solution.py:28
  59.0 133.9 %all-gather.17.cloned.1.call-start = ((), (), s32[]{:S(2)}) async-start(), calls=%async_computation.5 | async-start | bytes 1572864 | tf_op jit(solution)/shard_map/all_gather | solution.py:51
  104.6 228.4 %all-gather.13.cloned.1.call-start = ((), (), s32[]{:S(2)}) async-start(), calls=%async_computation.3 | async-start | bytes 4227072 | tf_op jit(solution)/shard_map/all_gather | solution.py:23
  105.0 94.1 %copy-start.5 = (f32[128]{0:T(128)}, f32[128]{0:T(128)S(1)}, u32[]{:S(2)}) copy-start(f32[128]{0:T(128)S(1)} %add_rsqrt_fusion) | copy-start | bytes 1540
  105.3 93.7 %copy-start.1 = (bf16[128,2048]{0,1:T(8,128)(2,1)}, bf16[128,2048]{0,1:T(8,128)(2,1)S(1)}, u32[]{:S(2)}) copy-start(bf16[128,2048]{0,1:T(8,128)(2,1)S(1)} %fusion.80) | copy-start | bytes 1572868
  196.8 7.0 collective-permute-start
  341.7 3.2 copy-start.2
  725.1 2.5 copy-start
  731.0 14.2 %all-to-all-start.1 = ((bf16[4,128,512]{2,1,0:T(8,128)(2,1)}), bf16[4,128,512]{2,1,0:T(8,128)(2,1)S(1)}, u32[]{:S(2)}, u32[]{:S(2)}) async-start(bf16[4,128,512]{2,1,0:T(8,128)(2,1)} %bitcast.135), calls=%async_computation.1 | async-start | bytes 1048576 | tf_op jit(solution)/shard_map/all_to_all | solution.py:70
Sparse Core Ops, SparseCore 0:
  11.6 138.5 all-gather.10
  152.3 17.5 all-gather.14
  172.0 20.8 all-gather.16
  196.3 136.6 all-gather.12
where the time goes:
time: 757 us; the launch traced here: 752 us
  matrix products  270 us (36%)
  waiting for transfers between devices  220 us (29%)
  other arithmetic  102 us (13%)
  blocking collectives  89.3 us (12%)
  local copies, waits for them, and re-layouts  40.8 us (5%)
  between operations  14 us (2%)
  starting transfers between devices  11.1 us (1%)
    dot_general x64, matrix products, head_scores(): jnp.einsum('qd,kd->qk', query_head, key_rows, preferred_element_type=jnp....  183 us
    all_gather x2, waiting for transfers between devices, side_by_side(): lax.all_gather(both, axis, axis=dim, tiled=True)  173 us
    all_gather x4, blocking collectives, gather_in_order(): parts = lax.all_gather(parts, axes[k])  89.3 us
    another operation x128, other arithmetic  83.1 us
    dot_general x64, matrix products, work(): jnp.dot(stick, value_rows, preferred_element_type=jnp.float32)  76.2 us
    all_gather x2, waiting for transfers between devices, gather_in_order(): parts = lax.all_gather(parts, axes[k])  35.2 us
  transfers between devices with their start and end apart: 7, of which 6 were waited for; matrix products, arithmetic and copies ran while one was open for 2% of the time, Pallas kernels for 0%

commit v1 on v0

v1 whole, which is shorter than its diff:
```python
import functools

import jax
import jax.numpy as jnp
from jax import lax
from jax.experimental import pallas as pl
from jax.experimental.pallas import tpu as pltpu
from jax.sharding import Mesh
from jax.sharding import PartitionSpec as P

D = 2048
HEAD = 64
CONV_K = 3
SP = ("sp_0", "sp_1", "sp_2")
KEYS = 256
EPS = 1e-06
FLOOR = 0.02
MESH = pl.DeviceIdType.MESH


def gather_kernel(nz, in_ref, out_ref, zs, zr, xs, xr, ps, pr):
    z, x, c = (lax.axis_index(a) for a in SP)
    nx = 4
    ups, downs = nz // 2, (nz - 1) // 2
    z_up, z_down = {"sp_0": lax.rem(z + 1, nz)}, {"sp_0": lax.rem(z + nz - 1, nz)}
    x_up, x_down = {"sp_1": lax.rem(x + 1, nx)}, {"sp_1": lax.rem(x + nx - 1, nx)}
    partner = {"sp_2": 1 - c}
    barrier = pltpu.get_barrier_semaphore()
    for peer in (z_up, z_down, x_up, x_down, partner):
        pl.semaphore_signal(barrier, inc=1, device_id=peer, device_id_type=MESH)
    pl.semaphore_wait(barrier, 5)

    def plane(dz):
        return lax.rem(z + dz + nz, nz)

    def column(dx):
        return lax.rem(x + dx + nx, nx)

    def index_of(dz):
        return -dz if dz <= 0 else ups + dz

    def copy(src, dst, ssem, rsem, peer):
        return pltpu.make_async_remote_copy(
            src_ref=src, dst_ref=dst, send_sem=ssem, recv_sem=rsem, device_id=peer, device_id_type=MESH
        )

    out_ref[z, x, c] = in_ref[...]
    sends = []

    def send(src, dst, ssem, rsem, peer):
        one = copy(src, dst, ssem, rsem, peer)
        one.start()
        sends.append(one)

    def await_block(slot, ssem, rsem, peer):
        copy(slot, slot, ssem, rsem, peer).wait_recv()

    def new_at(step):
        if step == 0:
            return [0]
        return ([-step] if step <= ups else []) + ([step] if 0 < step <= downs else [])

    for step in range(ups + 3):
        for dz in new_at(step):
            k = index_of(dz)
            slot = out_ref.at[plane(dz), x, c]
            if dz < 0:
                await_block(slot, zs.at[k], zr.at[k], z_down)
            elif dz > 0:
                await_block(slot, zs.at[k], zr.at[k], z_up)
            src = in_ref if dz == 0 else slot
            if dz <= 0 and step < ups:
                n = index_of(dz - 1)
                send(src, slot, zs.at[n], zr.at[n], z_up)
            if dz >= 0 and step < downs:
                n = index_of(dz + 1)
                send(src, slot, zs.at[n], zr.at[n], z_down)
            send(src, slot, xs.at[k, 0], xr.at[k, 0], x_up)
            send(src, slot, xs.at[k, 1], xr.at[k, 1], x_down)
        for dz in new_at(step - 1) if step >= 1 else []:
            k = index_of(dz)
            left = out_ref.at[plane(dz), column(-1), c]
            right = out_ref.at[plane(dz), column(1), c]
            await_block(left, xs.at[k, 0], xr.at[k, 0], x_down)
            await_block(right, xs.at[k, 1], xr.at[k, 1], x_up)
            if dz <= 0:
                send(left, left, xs.at[k, 2], xr.at[k, 2], x_up)
            else:
                send(right, right, xs.at[k, 2], xr.at[k, 2], x_down)
        for dz in new_at(step - 2) if step >= 2 else []:
            k = index_of(dz)
            far = out_ref.at[plane(dz), column(2), c]
            await_block(far, xs.at[k, 2], xr.at[k, 2], x_down if dz <= 0 else x_up)
            row = out_ref.at[plane(dz), :, c]
            send(row, row, ps.at[k], pr.at[k], partner)
    for k, dz in enumerate([*range(0, -ups - 1, -1), *range(1, downs + 1)]):
        row = out_ref.at[plane(dz), :, 1 - c]
        await_block(row, ps.at[k], pr.at[k], partner)
    for one in sends:
        one.wait_send()


def gather(block, nz, collective_id):
    rows, cols = block.shape
    dma = pltpu.SemaphoreType.DMA
    return pl.pallas_call(
        functools.partial(gather_kernel, nz),
        name="gather_sp",
        out_shape=jax.ShapeDtypeStruct((nz, 4, 2, rows, cols), block.dtype),
        in_specs=[pl.BlockSpec(memory_space=pltpu.VMEM)],
        out_specs=pl.BlockSpec(memory_space=pltpu.VMEM),
        scratch_shapes=[dma((nz,)), dma((nz,)), dma((nz, 3)), dma((nz, 3)), dma((nz,)), dma((nz,))],
        compiler_params=pltpu.CompilerParams(collective_id=collective_id, has_side_effects=True),
    )(block).reshape(-1, cols)


def sweep_kernel(bias_ref, q_ref, kv_ref, tri_ref, o_ref, s_ref):
    me = (lax.axis_index(SP[0]) * 4 + lax.axis_index(SP[1])) * 2 + lax.axis_index(SP[2])
    heads = bias_ref.shape[0]
    rows = q_ref.shape[0] // heads
    o_ref[...] = jnp.zeros_like(o_ref)
    s_ref[...] = jnp.zeros_like(s_ref)

    def block(begin, masked):
        kv = kv_ref[pl.ds(begin, KEYS), :]
        for h in range(heads):
            part = pl.ds(h * rows, rows)
            score = (
                lax.dot_general(
                    q_ref[part, :], kv, (((1,), (1,)), ((), ())), preferred_element_type=jnp.float32
                )
                + bias_ref[h]
            )
            if masked:
                key_pos = begin + lax.broadcasted_iota(jnp.int32, score.shape, 1)
                query_pos = me * rows + lax.broadcasted_iota(jnp.int32, score.shape, 0)
                score = jnp.where(key_pos < query_pos, score, -1e30)
            soft = jnp.log(1.0 + jnp.exp(-jnp.abs(score)))
            fail = jnp.maximum(score, 0.0) + soft
            high = fail.astype(jnp.bfloat16)
            low = (fail - high.astype(jnp.float32)).astype(jnp.bfloat16)
            tri = tri_ref[...]
            later = jnp.dot(high, tri, preferred_element_type=jnp.float32) + jnp.dot(
                low, tri, preferred_element_type=jnp.float32
            )
            stick = jnp.exp(jnp.minimum(score, 0.0) - soft - later).astype(jnp.bfloat16)
            out = jnp.dot(stick, kv, preferred_element_type=jnp.float32)
            gone = s_ref[part, :]
            o_ref[part, :] += jnp.exp(-gone) * out
            s_ref[part, :] = gone + (later[:, :1] + fail[:, :1])

    per_turn = 2 * KEYS // rows
    turns = lax.div(me, per_turn)
    for half in (1, 0):
        block(pl.multiple_of(turns * 2 * KEYS + half * KEYS, KEYS), True)

    @pl.loop(0, turns)
    def _(turn):
        for half in (1, 0):
            block(pl.multiple_of((turns - 1 - turn) * 2 * KEYS + half * KEYS, KEYS), False)


def sweep(query, all_kv, sb_bias):
    tokens, heads = query.shape[0], query.shape[1] // HEAD
    q = (query * HEAD ** (-0.5)).astype(jnp.bfloat16).reshape(tokens, heads, HEAD).transpose(1, 0, 2)
    q = jnp.pad(q.reshape(heads * tokens, HEAD), ((0, 0), (0, HEAD)))
    order = jnp.arange(KEYS)
    tri = (order[:, None] > order[None, :]).astype(jnp.bfloat16)
    vmem = pl.BlockSpec(memory_space=pltpu.VMEM)
    wide = jax.ShapeDtypeStruct((heads * tokens, 2 * HEAD), jnp.float32)
    out, gone = pl.pallas_call(
        sweep_kernel,
        name="sweep",
        out_shape=(wide, wide),
        in_specs=[pl.BlockSpec(memory_space=pltpu.SMEM), vmem, vmem, vmem],
        out_specs=(vmem, vmem),
    )(sb_bias, q, all_kv, tri)
    attended = out[:, HEAD:].astype(jnp.bfloat16).reshape(heads, tokens, HEAD)
    survival = -gone[:, 0].reshape(heads, tokens)
    return attended.transpose(1, 0, 2).reshape(tokens, heads * HEAD), survival


def copy_for_each(value, axis):
    copies = jnp.broadcast_to(value, (lax.axis_size(axis), *value.shape))
    return lax.all_to_all(copies, axis, split_axis=0, concat_axis=0, tiled=True)


def collect(value, axis):
    parts = copy_for_each(value, axis)
    return jnp.moveaxis(parts, 0, 1).reshape(value.shape[0], -1)


def from_behind(value, axis, steps):
    count = lax.axis_size(axis)
    return lax.ppermute(value, axis, [(source, source + steps) for source in range(count - steps)])


def summed_on_arrival(value, axis):
    size = lax.axis_size(axis)
    rows, cols = value.shape
    parts = jnp.moveaxis(value.reshape(rows, size, cols // size), 1, 0)
    parts = lax.all_to_all(parts, axis, 0, 0, tiled=True)
    return jnp.sum(parts.astype(jnp.float32), axis=0)


def local(
    stream,
    norm_gain,
    w_query,
    w_key,
    w_value,
    w_conv_in,
    w_conv_gate,
    conv_taps,
    sb_bias,
    w_out_attn,
    w_out_conv,
):
    tokens = stream.shape[0]
    nz = lax.axis_size(SP[0])
    ins = (w_key, w_value, w_query, w_conv_in, w_conv_gate)
    held = jnp.concatenate([*ins, w_out_attn.T, w_out_conv.T], axis=1)
    weights = gather(held, nz, 0)
    piece_f = collect(stream, "tp").astype(jnp.float32)
    scaled = (piece_f * norm_gain[None, :]).astype(jnp.bfloat16)
    row_scale = lax.rsqrt(jnp.sum(piece_f * piece_f, axis=1) / D + EPS)[:, None]
    ends, at = [], 0
    for w in ins:
        at += w.shape[1]
        ends.append(at)
    sums = jnp.dot(scaled, weights[:, :at], preferred_element_type=jnp.float32)
    mine = (sums * row_scale).astype(jnp.bfloat16)
    kv = mine[:, : ends[1]]
    query, conv_in, conv_gate = jnp.split(mine[:, ends[1] :], [e - ends[1] for e in ends[2:4]], axis=1)
    all_kv = gather(kv, nz, 1)
    previous = from_behind(conv_in[tokens - (CONV_K - 1) :], SP, 1)
    padded = jnp.concatenate([previous, conv_in], axis=0).astype(jnp.float32)
    conv_mixed = jnp.zeros((tokens, conv_in.shape[1]), jnp.float32)
    for tap in range(CONV_K):
        conv_mixed = conv_mixed + conv_taps[tap][None, :] * padded[tap : tap + tokens]
    conv_out = (conv_gate.astype(jnp.float32) * conv_mixed).astype(jnp.bfloat16)
    attended, survs = sweep(query, all_kv, sb_bias)
    log_weight_sum = jnp.log(jnp.maximum(-jnp.expm1(survs), FLOOR))
    partial_value = lax.dot_general(
        jnp.concatenate([attended, conv_out], axis=1),
        weights[:, at:],
        (((1,), (1,)), ((), ())),
        preferred_element_type=jnp.float32,
    )
    mixed = summed_on_arrival(partial_value.astype(jnp.bfloat16), "tp").astype(jnp.bfloat16)
    return (mixed, log_weight_sum)


def solution(mesh):
    torus = Mesh(
        mesh.devices.reshape(mesh.shape["sp"] // 8, 4, 2, mesh.shape["tp"]),
        ("sp_0", "sp_1", "sp_2", "tp"),
    )
    return jax.shard_map(
        local,
        mesh=torus,
        in_specs=(
            P(SP, "tp"),
            P(),
            P(SP, "tp"),
            P(SP, "tp"),
            P(SP, "tp"),
            P(SP, "tp"),
            P(SP, "tp"),
            P(None, "tp"),
            P("tp"),
            P("tp", SP),
            P("tp", SP),
        ),
        out_specs=(P(SP, "tp"), P("tp", SP)),
        check_vma=False,
    )
```

time: 757 us -> 216 us (0.29)
  the two profiles are of different devices: /device:TPU:480 before, /device:TPU:486 now
where the time goes in v1:
time: 216 us; the launch traced here: 215 us
  Pallas kernels  178 us (82%)
  starting transfers between devices  11.6 us (5%)
  waiting for transfers between devices  9.36 us (4%)
  local copies, waits for them, and re-layouts  7.11 us (3%)
  matrix products  5.19 us (2%)
  other arithmetic  2.95 us (1%)
    pallas_call x1, Pallas kernels, sweep(): pl.pallas_call(sweep_kernel, name='sweep', out_shape=(wide, wide), in_spe...  98.4 us
    pallas_call x2, Pallas kernels, gather(): pl.pallas_call(functools.partial(gather_kernel, nz), name='gather_sp', ou...  80 us
    all_to_all x1, waiting for transfers between devices, summed_on_arrival(): parts = lax.all_to_all(parts, axis, 0, 0, tiled=True)  9.35 us
    all_to_all x1, starting transfers between devices, summed_on_arrival(): parts = lax.all_to_all(parts, axis, 0, 0, tiled=True)  4.74 us
    all_to_all x1, starting transfers between devices, copy_for_each(): return lax.all_to_all(copies, axis, split_axis=0, concat_axis=0, tiled=True)  4.46 us
  transfers between devices with their start and end apart: 3, of which 1 were waited for; matrix products, arithmetic and copies ran while one was open for 3% of the time, Pallas kernels for 83%

profile of v1, /device:TPU:486, one launch (start us, length us, event | category | flops | bytes accessed | tf_op | source)
XLA Modules:
  0.0 215.4 jit_solution(15584761794342118391)
XLA Ops:
  0.6 0.0 copy-start.2
  0.6 0.0 copy-start.1
  0.6 1.0 copy.26
  1.7 0.9 broadcast_in_dim.2
  2.6 4.5 %all-to-all-start = ((bf16[4,128,512]{1,2,0:T(8,128)(2,1)}), bf16[4,128,512]{1,2,0:T(8,128)(2,1)S(1)}, u32[]{:S(2)}, u32[]{:S(2)}) async-start(bf16[4,128,512]{1,2,0:T(8,128)(2,1)} %broadcast_in_dim.2), calls=%async_computation | async-start | bytes 1048576 | tf_op jit(solution)/shard_map/all_to_all | solution.py:185
  7.0 1.5 concatenate.9.in_ref
  8.5 40.2 %gather_sp.2 = bf16[16,4,2,16,1408]{4,3,2,1,0:T(8,128)(2,1)} custom-call(bf16[16,1408]{1,0:T(8,128)(2,1)} %concatenate.9.in_ref), custom_call_target="tpu_custom_call" | custom-call | tf_op jit(solution)/shard_map/gather_sp/pallas_call | solution.py:106
  48.7 0.7 fusion.10.tri_ref
  49.4 0.0 copy-done.2
  49.4 0.0 all-to-all-done
  49.4 0.3 multiply_reduce_fusion
  49.7 0.0 copy-done.1
  49.7 0.3 fusion.9
  50.1 2.8 %fusion.6 = bf16[128,896]{1,0:T(8,128)(2,1)S(1)} fusion(bf16[128,2048]{0,1:T(8,128)(2,1)S(1)} %fusion.9, bf16[2048,1408]{1,0:T(8,128)(2,1)} %bitcast.31, f32[128]{0:T(128)S(1)} %add_rsqrt_fusion), kind=kOutput, calls=%fused_computation.5 | convolution fusion | flops 469991424 | bytes 4424192 | tf_op jit(solution)/shard_map/dot_general | solution.py:231
  52.9 2.4 %collective-permute-start = (bf16[2,256]{1,0:T(2,128)(2,1)S(1)}, bf16[2,256]{1,0:T(2,128)(2,1)S(1)}, u32[]{:S(2)}, u32[]{:S(2)}) collective-permute-start(bf16[2,256]{1,0:T(2,128)(2,1)S(1)} %slice.57), channel_id=1, source_target_pairs={{0,4},{4,8},{8,12},{12,16},{16,20},{20,24},{24,28},{28,32},{32,36}... | collective-permute-start | bytes 3080 | tf_op jit(solution)/shard_map/ppermute | solution.py:195
  55.3 0.6 slice.55.in_ref
  55.9 0.1 copy.27
  56.0 0.1 copy.28
  56.2 39.8 %gather_sp.3 = bf16[16,4,2,128,128]{4,3,2,1,0:T(8,128)(2,1)} custom-call(bf16[128,128]{1,0:T(8,128)(2,1)} %slice.55.in_ref), custom_call_target="tpu_custom_call" | custom-call | tf_op jit(solution)/shard_map/gather_sp/pallas_call | solution.py:106
  96.0 0.7 pad.4.q_ref
  96.7 98.4 %sweep.1 = (f32[512,128]{1,0:T(8,128)}, f32[512,128]{1,0:T(8,128)}) custom-call(f32[4]{0:T(128)} %bias_ref.1, bf16[512,128]{1,0:T(8,128)(2,1)} %pad.4.q_ref, bf16[16384,128]{1,0:T(8,128)(2,1)} %bitcast.30, bf16[256,256]{1,0:T(8,128)(2,1)} %fusion.10.tri_ref), custom_call_target="tpu_custom_call" | custom-call | tf_op jit(solution)/shard_map/sweep/pallas_call | solution.py:171
  195.1 1.1 slice.87
  196.2 0.1 copy.29
  196.3 0.1 copy.30
  196.4 0.0 collective-permute-done
  196.5 0.1 fusion.13
  196.5 2.4 %convolution_convert_fusion = bf16[128,2048]{1,0:T(8,128)(2,1)S(1)} fusion(bf16[2048,1408]{1,0:T(8,128)(2,1)} %bitcast.32, bf16[128,256]{1,0:T(8,128)(2,1)S(1)} %fusion.13, bf16[128,256]{1,0:T(8,128)(2,1)S(1)} %copy.30), kind=kOutput, calls=%fused_computation.2 | convolution fusion | flops 268959744 | bytes 2752512 | tf_op jit(solution)/shard_map/dot_general | solution.py:244
  198.9 0.8 copy.34
  199.8 4.7 %all-to-all-start.1 = ((bf16[4,128,512]{2,1,0:T(8,128)(2,1)}), bf16[4,128,512]{2,1,0:T(8,128)(2,1)S(1)}, u32[]{:S(2)}, u32[]{:S(2)}) async-start(bf16[4,128,512]{2,1,0:T(8,128)(2,1)} %bitcast.29), calls=%async_computation.1 | async-start | bytes 1048576 | tf_op jit(solution)/shard_map/all_to_all | solution.py:202
  204.5 0.8 log_reduce_fusion
  205.3 9.4 %all-to-all-done.1 = bf16[4,128,512]{2,1,0:T(8,128)(2,1)S(1)} async-done(((bf16[4,128,512]{2,1,0:T(8,128)(2,1)}), bf16[4,128,512]{2,1,0:T(8,128)(2,1)S(1)}, u32[]{:S(2)}, u32[]{:S(2)}) %all-to-all-start.1) | async-done | bytes 524320 | tf_op jit(solution)/shard_map/all_to_all | solution.py:202
  214.6 0.7 reduce_sum.22
  (7 shorter events, 0.1 us)
Async XLA Ops:
  0.6 48.8 %copy-start.2 = (f32[3,256]{1,0:T(4,128)S(1)}, f32[3,256]{1,0:T(4,128)}, u32[]{:S(2)}) copy-start(f32[3,256]{1,0:T(4,128)} %param.18) | copy-start | bytes 9220
  0.6 49.1 %copy-start.1 = (f32[2048]{0:T(1024)S(1)}, f32[2048]{0:T(1024)}, u32[]{:S(2)}) copy-start(f32[2048]{0:T(1024)} %param.12) | copy-start | bytes 24580
  2.6 46.9 %all-to-all-start = ((bf16[4,128,512]{1,2,0:T(8,128)(2,1)}), bf16[4,128,512]{1,2,0:T(8,128)(2,1)S(1)}, u32[]{:S(2)}, u32[]{:S(2)}) async-start(bf16[4,128,512]{1,2,0:T(8,128)(2,1)} %broadcast_in_dim.2), calls=%async_computation | async-start | bytes 1048576 | tf_op jit(solution)/shard_map/all_to_all | solution.py:185
  52.9 143.6 %collective-permute-start = (bf16[2,256]{1,0:T(2,128)(2,1)S(1)}, bf16[2,256]{1,0:T(2,128)(2,1)S(1)}, u32[]{:S(2)}, u32[]{:S(2)}) collective-permute-start(bf16[2,256]{1,0:T(2,128)(2,1)S(1)} %slice.57), channel_id=1, source_target_pairs={{0,4},{4,8},{8,12},{12,16},{16,20},{20,24},{24,28},{28,32},{32,36}... | collective-permute-start | bytes 3080 | tf_op jit(solution)/shard_map/ppermute | solution.py:195
  195.1 9.4 %copy-start = (f32[512,128]{1,0:T(8,128)S(1)}, f32[512,128]{1,0:T(8,128)}, u32[]{:S(2)}) copy-start(f32[512,128]{1,0:T(8,128)} %get-tuple-element.5) | copy-start | bytes 786436
  199.8 14.9 %all-to-all-start.1 = ((bf16[4,128,512]{2,1,0:T(8,128)(2,1)}), bf16[4,128,512]{2,1,0:T(8,128)(2,1)S(1)}, u32[]{:S(2)}, u32[]{:S(2)}) async-start(bf16[4,128,512]{2,1,0:T(8,128)(2,1)} %bitcast.29), calls=%async_computation.1 | async-start | bytes 1048576 | tf_op jit(solution)/shard_map/all_to_all | solution.py:202

commit v2 on v1

v2 whole, which is shorter than its diff:
```python
import functools

import jax
import jax.numpy as jnp
from jax import lax
from jax.experimental import pallas as pl
from jax.experimental.pallas import tpu as pltpu
from jax.sharding import Mesh
from jax.sharding import PartitionSpec as P

HEAD = 64
SP = ("sp_0", "sp_1", "sp_2")
KEYS = 256
EPS = 1e-06
FLOOR = 0.02
LN2 = 0.6931471805599453
NT = (((1,), (1,)), ((), ()))
MESH = pl.DeviceIdType.MESH


class Spread:
    def __init__(self, nz, own, buf, zs, zr, xs, xr, ps, pr):
        self.nz, self.own, self.buf = nz, own, buf
        self.zs, self.zr, self.xs, self.xr, self.ps, self.pr = zs, zr, xs, xr, ps, pr
        self.z, self.x, self.c = (lax.axis_index(a) for a in SP)
        self.ups, self.downs = nz // 2, (nz - 1) // 2
        self.z_up, self.z_down = ({"sp_0": lax.rem(self.z + d, nz)} for d in (1, nz - 1))
        self.x_up, self.x_down = ({"sp_1": lax.rem(self.x + d, 4)} for d in (1, 3))
        self.partner = {"sp_2": 1 - self.c}
        self.peers = (self.z_up, self.z_down, self.x_up, self.x_down, self.partner)

    def plane(self, up, n):
        return lax.rem(self.z - n + self.nz, self.nz) if up else lax.rem(self.z + n, self.nz)

    def slot(self, up, n, dx=0):
        return self.buf.at[self.plane(up, n), lax.rem(self.x + dx, 4), self.c]

    def index(self, up, n):
        return n if up else self.ups + n

    def on_z(self, up, n, src=None):
        k, slot = self.index(up, n), self.slot(up, n)
        return remote(slot if src is None else src, slot, self.zs.at[k], self.zr.at[k], self.z_up if up else self.z_down)

    def passed_on(self, up, n, src):
        k, slot = self.index(up, n + 1), self.slot(up, n)
        return remote(src, slot, self.zs.at[k], self.zr.at[k], self.z_up if up else self.z_down)

    def along_x(self, up, n, way, src=None):
        k, slot = self.index(up, n), self.slot(up, n)
        peer = self.x_up if way == 0 else self.x_down
        return remote(slot if src is None else src, slot, self.xs.at[k, way], self.xr.at[k, way], peer)

    def far_x(self, up, n):
        k, slot = self.index(up, n), self.slot(up, n, 3 if up else 1)
        return remote(slot, slot, self.xs.at[k, 2], self.xr.at[k, 2], self.x_up if up else self.x_down)

    def across(self, up, n, core):
        k, row = self.index(up, n), self.buf.at[self.plane(up, n), :, core]
        return remote(row, row, self.ps.at[k], self.pr.at[k], self.partner)

    def each(self, n, work):
        when(n <= self.ups, lambda: work(True))
        when(n <= self.downs, lambda: work(False))

    def begin(self):
        own = self.own
        self.passed_on(True, 0, own).start()
        if self.downs:
            self.passed_on(False, 0, own).start()
        self.along_x(True, 0, 0, own).start()
        self.along_x(True, 0, 1, own).start()
        self.buf[self.z, self.x, self.c] = own[...]

    def step_z(self, n):
        def work(up):
            self.on_z(up, n).wait_recv()
            when(n < (self.ups if up else self.downs), lambda: self.passed_on(up, n, self.slot(up, n)).start())
            for way in (0, 1):
                self.along_x(up, n, way).start()

        self.each(n, work)

    def step_x(self, n, first=False):
        def work(up):
            for way in (0, 1):
                self.along_x(up, n, way).wait_recv()
            self.far_x(up, n).start()

        work(True) if first else self.each(n, work)

    def step_far(self, n, first=False):
        def work(up):
            self.far_x(up, n).wait_recv()
            self.across(up, n, self.c).start()

        work(True) if first else self.each(n, work)

    def step_across(self, n, first=False):
        def work(up):
            self.across(up, n, 1 - self.c).wait_recv()

        work(True) if first else self.each(n, work)

    def finish(self):
        for k in range(self.nz):
            up = k <= self.ups
            n = k if up else k - self.ups
            if k:
                self.on_z(up, n).wait_send()
            for way in (0, 1):
                self.along_x(up, n, way).wait_send()
            self.far_x(up, n).wait_send()
            self.across(up, n, self.c).wait_send()


def remote(src, dst, ssem, rsem, peer):
    return pltpu.make_async_remote_copy(
        src_ref=src, dst_ref=dst, send_sem=ssem, recv_sem=rsem, device_id=peer, device_id_type=MESH
    )


def when(cond, work):
    if isinstance(cond, bool):
        if cond:
            work()
    else:
        pl.when(cond)(work)


def greet(peers):
    barrier = pltpu.get_barrier_semaphore()
    for peer in peers:
        pl.semaphore_signal(barrier, inc=1, device_id=peer, device_id_type=MESH)
    pl.semaphore_wait(barrier, len(peers))


def gather_kernel(nz, in_ref, out_ref, *sems):
    net = Spread(nz, in_ref, out_ref, *sems)
    greet(net.peers)
    net.begin()
    for step in range(1, net.ups + 6):
        net.step_z(step)
        if step >= 2:
            net.step_x(step - 2, step == 2)
        if step >= 4:
            net.step_far(step - 4, step == 4)
    for step in range(net.ups + 1):
        net.step_across(step, step == 0)
    net.finish()


def spread_sems(nz):
    dma = pltpu.SemaphoreType.DMA
    return [dma((nz,)), dma((nz,)), dma((nz, 3)), dma((nz, 3)), dma((nz,)), dma((nz,))]


def gather(block, nz, collective_id):
    rows, cols = block.shape
    return pl.pallas_call(
        functools.partial(gather_kernel, nz),
        name="gather_sp",
        out_shape=jax.ShapeDtypeStruct((nz, 4, 2, rows, cols), block.dtype),
        in_specs=[pl.BlockSpec(memory_space=pltpu.VMEM)],
        out_specs=pl.BlockSpec(memory_space=pltpu.VMEM),
        scratch_shapes=spread_sems(nz),
        compiler_params=pltpu.CompilerParams(collective_id=collective_id, has_side_effects=True),
    )(block).reshape(-1, cols)


def attend_kernel(
    nz, nt, bias_ref, q_ref, own_ref, conv_ref, gate_ref, taps_ref, tri_ref, mixed_ref, weight_ref,
    buf, halo, o_new, s_new, o_old, s_old, part, heard, zs, zr, xs, xr, ps, pr, hs, hr, ys, yr,
):
    net = Spread(nz, own_ref, buf, zs, zr, xs, xr, ps, pr)
    me = (net.z * 4 + net.x) * 2 + net.c
    y = lax.axis_index("tp")
    heads = bias_ref.shape[0]
    rows = q_ref.shape[0] // heads
    total = nz * 8

    def device(index):
        return {"sp_0": lax.div(index, 8), "sp_1": lax.rem(lax.div(index, 2), 4), "sp_2": lax.rem(index, 2)}

    ahead, behind = device(lax.rem(me + 1, total)), device(lax.rem(me + total - 1, total))
    others = [{"tp": lax.rem(y + r, nt)} for r in range(1, nt)]
    greet((*net.peers, ahead, behind, *others))
    net.begin()
    tail = remote(conv_ref.at[pl.ds(rows - 16, 16), :], halo, hs, hr, ahead)
    tail.start()
    for ref in (o_new, s_new, o_old, s_old):
        ref[...] = jnp.zeros_like(ref)

    def sweep(at, masked):
        out, gone = None, None
        for i in (3, 2, 1, 0):
            kv = buf[at, i, :, pl.ds(0, rows), :].reshape(KEYS, 2 * HEAD)
            both = jnp.concatenate([kv[:, :HEAD], kv[:, :HEAD]], axis=1)
            score = lax.dot_general(q_ref[...], both, NT, preferred_element_type=jnp.float32)
            score = jnp.concatenate(
                [score[h * rows : (h + 1) * rows] + bias_ref[h] for h in range(heads)], axis=0
            )
            if masked:
                key_pos = i * KEYS + lax.broadcasted_iota(jnp.int32, score.shape, 1)
                query_pos = lax.rem(me, 8) * rows + lax.rem(
                    lax.broadcasted_iota(jnp.int32, score.shape, 0), rows
                )
                score = jnp.where(key_pos < query_pos, score, -1e30)
            fail = jnp.maximum(score, lax.log2(1.0 + jnp.exp2(jnp.minimum(score, 80.0))))
            later = jnp.dot(fail.astype(jnp.bfloat16), tri_ref[...], preferred_element_type=jnp.float32)
            power = (score - fail) - later
            block = later[:, :1] + fail[:, :1]
            if gone is None:
                gone = jnp.broadcast_to(block, (heads * rows, 2 * HEAD))
            else:
                power = power - jnp.concatenate([gone, gone], axis=1)
                gone = gone + block
            stick = jnp.exp2(power).astype(jnp.bfloat16)
            term = jnp.dot(stick, kv, preferred_element_type=jnp.float32)
            out = term if out is None else out + term
        return out, gone

    def take_new(n, masked=False):
        out, gone = sweep(net.plane(True, n), masked)
        before = s_new[...]
        o_new[...] += jnp.exp2(-before) * out
        s_new[...] = before + gone

    def take_old(n):
        out, gone = sweep(net.plane(False, n), False)
        o_old[...] = o_old[...] * jnp.exp2(-gone) + out
        s_old[...] += gone

    net.step_z(1)
    net.step_x(0, True)
    net.step_z(2)
    net.step_x(1)
    net.step_far(0, True)
    net.step_z(3)
    net.step_across(0, True)
    take_new(0, True)
    net.step_x(2)
    net.step_far(1)

    @pl.loop(1, net.ups + 1)
    def _(n):
        net.step_z(n + 3)
        net.step_across(n)
        pl.when(net.z - n >= 0)(lambda: take_new(n))
        net.step_x(n + 2)
        pl.when((net.z + n >= nz) & (n <= net.downs))(lambda: take_old(n))
        net.step_far(n + 1)

    gone = s_new[...]
    out = o_new[...] + jnp.exp2(-gone) * o_old[...]
    survived = (gone + s_old[...]) * LN2
    weight = jnp.log(jnp.maximum(1.0 - jnp.exp(-survived), FLOOR))
    diagonal = lax.broadcasted_iota(jnp.int32, (rows, rows), 0) == lax.broadcasted_iota(
        jnp.int32, (rows, rows), 1
    )
    for h in range(heads):
        weight_ref[pl.ds(h, 1), :] = jnp.sum(
            jnp.where(diagonal, weight[h * rows : (h + 1) * rows], 0.0), axis=0, keepdims=True
        )
    attended = [out[h * rows : (h + 1) * rows, HEAD:] for h in range(heads)]

    tail.wait_recv()
    now = conv_ref[...].astype(jnp.float32)
    last = halo[...].astype(jnp.float32) * jnp.where(me > 0, 1.0, 0.0)
    row = lax.broadcasted_iota(jnp.int32, now.shape, 0)
    one = jnp.where(row == 0, last[15:16], pltpu.roll(now, 1, 0))
    two = jnp.where(row == 0, last[14:15], jnp.where(row == 1, last[15:16], pltpu.roll(now, 2, 0)))
    conv = taps_ref[0:1, :] * two + taps_ref[1:2, :] * one + taps_ref[2:3, :] * now
    conv = gate_ref[...].astype(jnp.float32) * conv
    act = jnp.concatenate([*attended, conv], axis=1).astype(jnp.bfloat16)

    share = nz // nt

    def project(to):
        planes = pl.ds(to * share, share)
        acc = None
        for j in range(4):
            w = buf[planes, :, :, pl.ds(rows + 16 * j, 16), :].reshape(share * 128, 128)
            term = lax.dot_general(
                act[:, 128 * j : 128 * (j + 1)], w, NT, preferred_element_type=jnp.float32
            )
            acc = term if acc is None else acc + term
        return acc.astype(jnp.bfloat16)

    sent = []
    for r in [*range(2, nt), 1] if nt > 1 else []:
        part[r] = project(lax.rem(y + r, nt))
        sent.append(remote(part.at[r], heard.at[r], ys.at[r], yr.at[r], others[r - 1]))
        sent[-1].start()
    mixed = project(y).astype(jnp.float32)
    for one_sent in sent:
        one_sent.wait_recv()
    for r in range(1, nt):
        mixed = mixed + heard[r].astype(jnp.float32)
    mixed_ref[...] = mixed.astype(jnp.bfloat16)
    for one_sent in sent:
        one_sent.wait_send()
    tail.wait_send()
    net.finish()


def attend(query, kv, w_out, conv_in, conv_gate, conv_taps, sb_bias, nz, nt):
    tokens, heads = query.shape[0], query.shape[1] // HEAD
    q = query.astype(jnp.float32).reshape(tokens, heads, HEAD).transpose(1, 0, 2) * (HEAD ** (-0.5) / LN2)
    q = q.reshape(heads * tokens, HEAD)
    high = lax.reduce_precision(q, 8, 7)
    q = jnp.concatenate([high, q - high], axis=1).astype(jnp.bfloat16)
    order = jnp.arange(KEYS)
    tri = (order[:, None] > order[None, :]).astype(jnp.bfloat16)
    cols = w_out.shape[0] // 4
    w_rows = w_out.reshape(4, cols, 16).transpose(0, 2, 1).reshape(64, cols)
    own = jnp.concatenate([kv, w_rows], axis=0)
    vmem = pl.BlockSpec(memory_space=pltpu.VMEM)
    out_cols = nz * 128 // nt
    wide = pltpu.VMEM((heads * tokens, 2 * HEAD), jnp.float32)
    parts = pltpu.VMEM((nt, tokens, out_cols), jnp.bfloat16)
    dma = pltpu.SemaphoreType.DMA
    return pl.pallas_call(
        functools.partial(attend_kernel, nz, nt),
        name="attend",
        out_shape=(
            jax.ShapeDtypeStruct((tokens, out_cols), jnp.bfloat16),
            jax.ShapeDtypeStruct((heads, tokens), jnp.float32),
        ),
        in_specs=[pl.BlockSpec(memory_space=pltpu.SMEM)] + [vmem] * 6,
        out_specs=(vmem, vmem),
        scratch_shapes=[
            pltpu.VMEM((nz, 4, 2, *own.shape), jnp.bfloat16),
            pltpu.VMEM((16, conv_in.shape[1]), jnp.bfloat16),
            *[wide] * 4,
            *[parts] * 2,
            *spread_sems(nz),
            dma,
            dma,
            dma((nt,)),
            dma((nt,)),
        ],
        compiler_params=pltpu.CompilerParams(collective_id=1, has_side_effects=True),
    )(sb_bias / LN2, q, own, conv_in, conv_gate, conv_taps, tri)


def copy_for_each(value, axis):
    copies = jnp.broadcast_to(value, (lax.axis_size(axis), *value.shape))
    return lax.all_to_all(copies, axis, split_axis=0, concat_axis=0, tiled=True)


def collect(value, axis):
    parts = copy_for_each(value, axis)
    return jnp.moveaxis(parts, 0, 1).reshape(value.shape[0], -1)


def local(
    stream,
    norm_gain,
    w_query,
    w_key,
    w_value,
    w_conv_in,
    w_conv_gate,
    conv_taps,
    sb_bias,
    w_out_attn,
    w_out_conv,
):
    nz, nt = lax.axis_size(SP[0]), lax.axis_size("tp")
    ins = (w_key, w_value, w_query, w_conv_in, w_conv_gate)
    weights = gather(jnp.concatenate(ins, axis=1), nz, 0)
    piece_f = collect(stream, "tp").astype(jnp.float32)
    scaled = (piece_f * norm_gain[None, :]).astype(jnp.bfloat16)
    row_scale = lax.rsqrt(jnp.sum(piece_f * piece_f, axis=1) / piece_f.shape[1] + EPS)[:, None]
    sums = jnp.dot(scaled, weights, preferred_element_type=jnp.float32)
    mine = (sums * row_scale).astype(jnp.bfloat16)
    ends, at = [], w_key.shape[1]
    for w in ins[1:-1]:
        at += w.shape[1]
        ends.append(at)
    kv, query, conv_in, conv_gate = jnp.split(mine, ends, axis=1)
    w_out = jnp.concatenate([w_out_attn, w_out_conv], axis=0)
    return attend(query, kv, w_out, conv_in, conv_gate, conv_taps, sb_bias, nz, nt)


def solution(mesh):
    torus = Mesh(
        mesh.devices.reshape(mesh.shape["sp"] // 8, 4, 2, mesh.shape["tp"]),
        ("sp_0", "sp_1", "sp_2", "tp"),
    )
    return jax.shard_map(
        local,
        mesh=torus,
        in_specs=(
            P(SP, "tp"),
            P(),
            P(SP, "tp"),
            P(SP, "tp"),
            P(SP, "tp"),
            P(SP, "tp"),
            P(SP, "tp"),
            P(None, "tp"),
            P("tp"),
            P("tp", SP),
            P("tp", SP),
        ),
        out_specs=(P(SP, "tp"), P("tp", SP)),
        check_vma=False,
    )
```

time: 216 us -> 124 us (0.57)
  the two profiles are of different devices: /device:TPU:486 before, /device:TPU:1 now
where the time goes in v2:
time: 124 us; the launch traced here: 123 us
  Pallas kernels  103 us (83%)
  local copies, waits for them, and re-layouts  7.75 us (6%)
  starting transfers between devices  5 us (4%)
  other arithmetic  3.69 us (3%)
  matrix products  2.78 us (2%)
    pallas_call x1, Pallas kernels, attend(): pl.pallas_call(functools.partial(attend_kernel, nz, nt), name='attend', o...  53.9 us
    pallas_call x1, Pallas kernels, gather(): pl.pallas_call(functools.partial(gather_kernel, nz), name='gather_sp', ou...  49.2 us
    all_to_all x1, starting transfers between devices, copy_for_each(): return lax.all_to_all(copies, axis, split_axis=0, concat_axis=0, tiled=True)  5 us
    unnamed x5, local copies, waits for them, and re-layouts  3.84 us
    dot_general x1, matrix products, local(): sums = jnp.dot(scaled, weights, preferred_element_type=jnp.float32)  2.78 us
  transfers between devices with their start and end apart: 1, of which 0 were waited for; matrix products, arithmetic and copies ran while one was open for 3% of the time, Pallas kernels for 40%

profile of v2, /device:TPU:1, one launch (start us, length us, event | category | flops | bytes accessed | tf_op | source)
XLA Modules:
  0.0 123.0 jit_solution(7227923202205050729)
XLA Ops:
  0.6 0.0 copy-start
  0.6 1.0 copy.15
  1.7 0.9 broadcast_in_dim.2
  2.5 5.0 %all-to-all-start = ((bf16[4,128,512]{1,2,0:T(8,128)(2,1)}), bf16[4,128,512]{1,2,0:T(8,128)(2,1)S(1)}, u32[]{:S(2)}, u32[]{:S(2)}) async-start(bf16[4,128,512]{1,2,0:T(8,128)(2,1)} %broadcast_in_dim.2), calls=%async_computation | async-start | bytes 1048576 | tf_op jit(solution)/shard_map/all_to_all | solution.py:349
  7.5 0.7 copy_bitcast_fusion
  8.3 0.7 mul.37
  9.0 1.4 %concatenate.13.in_ref = bf16[16,896]{1,0:T(8,128)(2,1)} concatenate(bf16[16,64]{1,0:T(8,128)(2,1)} %param.14, bf16[16,64]{1,0:T(8,128)(2,1)} %param.15, bf16[16,256]{1,0:T(8,128)(2,1)} %param.13, bf16[16,256]{1,0:T(8,128)(2,1)} %param.16, bf16[16,256]{1,0:T(8,128)(2,1)} %param.17), dimensions={1} | concatenate | bytes 57344 | tf_op jit(solution)/shard_map/concatenate | solution.py:372
  10.4 49.2 %gather_sp.1 = bf16[16,4,2,16,896]{4,3,2,1,0:T(8,128)(2,1)} custom-call(bf16[16,896]{1,0:T(8,128)(2,1)} %concatenate.13.in_ref), custom_call_target="tpu_custom_call" | custom-call | tf_op jit(solution)/shard_map/gather_sp/pallas_call | solution.py:160
  59.6 0.7 fusion.4.tri_ref
  60.3 0.0 copy-done
  60.3 0.5 broadcast_multiply_fusion.bias_ref
  60.8 0.0 all-to-all-done
  60.8 0.3 fusion.2
  61.2 2.8 %fusion = bf16[128,896]{1,0:T(8,128)(2,1)S(1)} fusion(bf16[128,2048]{0,1:T(8,128)(2,1)S(1)} %bitcast.21, bf16[2048,896]{1,0:T(8,128)(2,1)} %bitcast.20, f32[128]{0:T(128)S(1)} %add_rsqrt_fusion), kind=kOutput, calls=%fused_computation.3 | convolution fusion | flops 469991424 | bytes 4424192 | tf_op jit(solution)/shard_map/dot_general | solution.py:376
  64.0 0.7 fusion.5
  64.7 0.1 copy.16
  64.7 0.1 copy.17
  64.9 0.8 pad_maximum_fusion.q_ref
  65.7 0.6 pad_maximum_fusion.1.own_ref
  66.3 53.9 %attend.1 = (bf16[128,512]{1,0:T(8,128)(2,1)}, f32[4,128]{1,0:T(4,128)}) custom-call(f32[4]{0:T(128)} %broadcast_multiply_fusion.bias_ref, bf16[512,128]{1,0:T(8,128)(2,1)} %pad_maximum_fusion.q_ref, bf16[192,128]{1,0:T(8,128)(2,1)} %pad_maximum_fusion.1.own_ref, bf16[128,256]{1,0:T(8,128)(2,1)} %get-tuple-element.7.conv_ref, ...), custom_call_target="tpu_custom_call" | custom-call | tf_op jit(solution)/shard_map/attend/pallas_call | solution.py:323
  120.2 1.6 %copy.23 = bf16[128,512]{1,0:T(8,128)(2,1)} copy(bf16[128,512]{1,0:T(8,128)(2,1)} %get-tuple-element.10) | data formatting | bytes 262144
  121.8 1.2 %copy.24 = f32[4,128]{1,0:T(4,128)} copy(f32[4,128]{1,0:T(4,128)} %get-tuple-element.11) | data formatting | bytes 4096
  (4 shorter events, 0.1 us)
Async XLA Ops:
  0.6 59.7 %copy-start = (f32[4]{0:T(128)S(1)}, f32[4]{0:T(128)}, u32[]{:S(2)}) copy-start(f32[4]{0:T(128)} %param.19) | copy-start | bytes 52
  2.5 58.3 %all-to-all-start = ((bf16[4,128,512]{1,2,0:T(8,128)(2,1)}), bf16[4,128,512]{1,2,0:T(8,128)(2,1)S(1)}, u32[]{:S(2)}, u32[]{:S(2)}) async-start(bf16[4,128,512]{1,2,0:T(8,128)(2,1)} %broadcast_in_dim.2), calls=%async_computation | async-start | bytes 1048576 | tf_op jit(solution)/shard_map/all_to_all | solution.py:349

commit v3 on v2

--- a/solution.py
+++ b/solution.py
@@ -19,15 +19,22 @@
 
 
 class Spread:
-    def __init__(self, nz, own, buf, zs, zr, xs, xr, ps, pr):
+    def __init__(self, nz, stride, own, buf, zs, zr, xs, xr, ps, pr):
         self.nz, self.own, self.buf = nz, own, buf
         self.zs, self.zr, self.xs, self.xr, self.ps, self.pr = zs, zr, xs, xr, ps, pr
         self.z, self.x, self.c = (lax.axis_index(a) for a in SP)
         self.ups, self.downs = nz // 2, (nz - 1) // 2
-        self.z_up, self.z_down = ({"sp_0": lax.rem(self.z + d, nz)} for d in (1, nz - 1))
+        self.stride = min(stride, self.ups)
         self.x_up, self.x_down = ({"sp_1": lax.rem(self.x + d, 4)} for d in (1, 3))
         self.partner = {"sp_2": 1 - self.c}
-        self.peers = (self.z_up, self.z_down, self.x_up, self.x_down, self.partner)
+        on_z = [self.z_peer(up, r) for r in range(1, self.stride + 1) for up in (True, False)]
+        self.peers = (*on_z, self.x_up, self.x_down, self.partner)
+
+    def z_peer(self, up, r):
+        return {"sp_0": lax.rem(self.z + r if up else self.z - r + self.nz, self.nz)}
+
+    def limit(self, up):
+        return self.ups if up else self.downs
 
     def plane(self, up, n):
         return lax.rem(self.z - n + self.nz, self.nz) if up else lax.rem(self.z + n, self.nz)
@@ -38,13 +45,16 @@
     def index(self, up, n):
         return n if up else self.ups + n
 
-    def on_z(self, up, n, src=None):
+    def pass_on(self, up, n, src):
+        for r in range(self.stride, 0, -1):
+            k, slot = self.index(up, n + r), self.slot(up, n)
+            sems = self.zs.at[k], self.zr.at[k]
+            go = lambda r=r, sems=sems: remote(src, slot, *sems, self.z_peer(up, r)).start()
+            when(n + r <= self.limit(up), go)
+
+    def on_z(self, up, n):
         k, slot = self.index(up, n), self.slot(up, n)
-        return remote(slot if src is None else src, slot, self.zs.at[k], self.zr.at[k], self.z_up if up else self.z_down)
-
-    def passed_on(self, up, n, src):
-        k, slot = self.index(up, n + 1), self.slot(up, n)
-        return remote(src, slot, self.zs.at[k], self.zr.at[k], self.z_up if up else self.z_down)
+        return remote(slot, slot, self.zs.at[k], self.zr.at[k], self.z_peer(up, 1))
 
     def along_x(self, up, n, way, src=None):
         k, slot = self.index(up, n), self.slot(up, n)
@@ -65,9 +75,8 @@
 
     def begin(self):
         own = self.own
-        self.passed_on(True, 0, own).start()
-        if self.downs:
-            self.passed_on(False, 0, own).start()
+        self.pass_on(True, 0, own)
+        self.pass_on(False, 0, own)
         self.along_x(True, 0, 0, own).start()
         self.along_x(True, 0, 1, own).start()
         self.buf[self.z, self.x, self.c] = own[...]
@@ -75,7 +84,7 @@
     def step_z(self, n):
         def work(up):
             self.on_z(up, n).wait_recv()
-            when(n < (self.ups if up else self.downs), lambda: self.passed_on(up, n, self.slot(up, n)).start())
+            when(n % self.stride == 0, lambda: self.pass_on(up, n, self.slot(up, n)))
             for way in (0, 1):
                 self.along_x(up, n, way).start()
 
@@ -135,44 +144,116 @@
     pl.semaphore_wait(barrier, len(peers))
 
 
-def gather_kernel(nz, in_ref, out_ref, *sems):
-    net = Spread(nz, in_ref, out_ref, *sems)
-    greet(net.peers)
-    net.begin()
-    for step in range(1, net.ups + 6):
-        net.step_z(step)
-        if step >= 2:
-            net.step_x(step - 2, step == 2)
-        if step >= 4:
-            net.step_far(step - 4, step == 4)
-    for step in range(net.ups + 1):
-        net.step_across(step, step == 0)
-    net.finish()
-
-
 def spread_sems(nz):
     dma = pltpu.SemaphoreType.DMA
     return [dma((nz,)), dma((nz,)), dma((nz, 3)), dma((nz, 3)), dma((nz,)), dma((nz,))]
 
 
-def gather(block, nz, collective_id):
-    rows, cols = block.shape
+def project_kernel(
+    nz, nt, own_ref, stream_ref, gain_ref, out_rows_ref, kv_ref, q_ref, conv_ref, gate_ref,
+    buf, heard, scaled, acc, zs, zr, xs, xr, ps, pr, ys, yr,
+):
+    net = Spread(nz, 4, own_ref, buf, zs, zr, xs, xr, ps, pr)
+    y = lax.axis_index("tp")
+    tokens = stream_ref.shape[0]
+    others = [{"tp": lax.rem(y + r, nt)} for r in range(1, nt)]
+    greet((*net.peers, *others))
+    net.begin()
+    sent = [
+        remote(stream_ref, heard.at[y], ys.at[r], yr.at[r], others[r - 1]) for r in (2, 1, 3) if r < nt
+    ]
+    for one in sent:
+        one.start()
+    heard[y] = stream_ref[...]
+    acc[...] = jnp.zeros_like(acc)
+    share = nz // nt
+
+    def scale():
+        for r in range(1, nt):
+            slot = heard.at[lax.rem(y + nt - r, nt)]
+            remote(slot, slot, ys.at[r], yr.at[r], others[r - 1]).wait_recv()
+        squares = jnp.zeros((tokens, 1), jnp.float32)
+        for b in range(nt):
+            piece = heard[b].astype(jnp.float32)
+            squares = squares + jnp.sum(piece * piece, axis=1, keepdims=True)
+            piece = (piece * gain_ref[b : b + 1, :]).astype(jnp.bfloat16)
+            for j in range(share):
+                scaled[b * share + j] = piece[:, 128 * j : 128 * (j + 1)]
+        return squares
+
+    def take(up, n):
+        at = net.plane(up, n)
+        rows = buf[at].reshape(128, acc.shape[1])
+        acc[...] += jnp.dot(scaled[at], rows, preferred_element_type=jnp.float32)
+
+    near = net.stride
+    order = [0, *(q + r for q in range(0, net.ups, near) for r in range(near, 0, -1))]
+    squares = None
+    for i in range(len(order) + 6):
+        if 0 < i < len(order):
+            net.step_z(order[i])
+        if 2 <= i < len(order) + 2:
+            net.step_x(order[i - 2], i == 2)
+        if 4 <= i < len(order) + 4:
+            net.step_far(order[i - 4], i == 4)
+        if 6 <= i:
+            n = order[i - 6]
+            if n == 0:
+                squares = scale()
+            net.step_across(n, n == 0)
+            take(True, n)
+            if 0 < n <= net.downs:
+                take(False, n)
+    row_scale = lax.rsqrt(squares / (nz * 128) + EPS)
+    mine = (acc[...] * row_scale).astype(jnp.bfloat16)
+    wide = conv_ref.shape[1]
+    heads = wide // HEAD
+    kv_ref[pl.ds(0, tokens), :] = mine[:, : 2 * HEAD]
+    kv_ref[pl.ds(tokens, 64), :] = out_rows_ref[...]
+    for h in range(heads):
+        begin = 2 * HEAD + h * HEAD
+        q = mine[:, begin : begin + HEAD].astype(jnp.float32) * (HEAD ** (-0.5) / LN2)
+        high = q.astype(jnp.bfloat16).astype(jnp.float32)
+        q_ref[pl.ds(h * tokens, tokens), :] = jnp.concatenate([high, q - high], axis=1).astype(jnp.bfloat16)
+    conv_ref[...] = mine[:, 2 * HEAD + wide : 2 * HEAD + 2 * wide]
+    gate_ref[...] = mine[:, 2 * HEAD + 2 * wide :]
+    for one in sent:
+        one.wait_send()
+    net.finish()
+
+
+def project(rows, stream, norm_gain, w_out, nz, nt):
+    tokens = stream.shape[0]
+    wide = (rows.shape[1] - 2 * HEAD) // 3
+    cols = w_out.shape[0] // 4
+    out_rows = w_out.reshape(4, cols, 16).transpose(0, 2, 1).reshape(64, cols)
+    vmem = pl.BlockSpec(memory_space=pltpu.VMEM)
+    dma = pltpu.SemaphoreType.DMA
+    shapes = [(tokens + 64, 2 * HEAD), (wide // HEAD * tokens, 2 * HEAD), (tokens, wide), (tokens, wide)]
     return pl.pallas_call(
-        functools.partial(gather_kernel, nz),
-        name="gather_sp",
-        out_shape=jax.ShapeDtypeStruct((nz, 4, 2, rows, cols), block.dtype),
-        in_specs=[pl.BlockSpec(memory_space=pltpu.VMEM)],
-        out_specs=pl.BlockSpec(memory_space=pltpu.VMEM),
-        scratch_shapes=spread_sems(nz),
-        compiler_params=pltpu.CompilerParams(collective_id=collective_id, has_side_effects=True),
-    )(block).reshape(-1, cols)
+        functools.partial(project_kernel, nz, nt),
+        name="project",
+        out_shape=[jax.ShapeDtypeStruct(s, jnp.bfloat16) for s in shapes],
+        in_specs=[vmem] * 4,
+        out_specs=[vmem] * 4,
+        scratch_shapes=[
+            pltpu.VMEM((nz, 4, 2, *rows.shape), jnp.bfloat16),
+            pltpu.VMEM((nt, *stream.shape), jnp.bfloat16),
+            pltpu.VMEM((nz, tokens, 128), jnp.bfloat16),
+            pltpu.VMEM((tokens, rows.shape[1]), jnp.float32),
+            *spread_sems(nz),
+            dma((nt,)),
+            dma((nt,)),
+        ],
+        compiler_params=pltpu.CompilerParams(collective_id=0, has_side_effects=True),
+    )(rows, stream, norm_gain.reshape(nt, -1), out_rows)
 
 
 def attend_kernel(
     nz, nt, bias_ref, q_ref, own_ref, conv_ref, gate_ref, taps_ref, tri_ref, mixed_ref, weight_ref,
     buf, halo, o_new, s_new, o_old, s_old, part, heard, zs, zr, xs, xr, ps, pr, hs, hr, ys, yr,
 ):
-    net = Spread(nz, own_ref, buf, zs, zr, xs, xr, ps, pr)
+    net = Spread(nz, 2, own_ref, buf, zs, zr, xs, xr, ps, pr)
     me = (net.z * 4 + net.x) * 2 + net.c
     y = lax.axis_index("tp")
     heads = bias_ref.shape[0]
@@ -231,25 +312,27 @@
         o_old[...] = o_old[...] * jnp.exp2(-gone) + out
         s_old[...] += gone
 
+    net.step_x(0, True)
     net.step_z(1)
-    net.step_x(0, True)
     net.step_z(2)
+    net.step_far(0, True)
     net.step_x(1)
-    net.step_far(0, True)
     net.step_z(3)
+    net.step_z(4)
     net.step_across(0, True)
     take_new(0, True)
     net.step_x(2)
     net.step_far(1)
+    net.step_x(3)
 
     @pl.loop(1, net.ups + 1)
     def _(n):
-        net.step_z(n + 3)
+        net.step_z(n + 4)
         net.step_across(n)
         pl.when(net.z - n >= 0)(lambda: take_new(n))
-        net.step_x(n + 2)
+        net.step_far(n + 1)
+        net.step_x(n + 3)
         pl.when((net.z + n >= nz) & (n <= net.downs))(lambda: take_old(n))
-        net.step_far(n + 1)
 
     gone = s_new[...]
     out = o_new[...] + jnp.exp2(-gone) * o_old[...]
@@ -304,17 +387,11 @@
     net.finish()
 
 
-def attend(query, kv, w_out, conv_in, conv_gate, conv_taps, sb_bias, nz, nt):
-    tokens, heads = query.shape[0], query.shape[1] // HEAD
-    q = query.astype(jnp.float32).reshape(tokens, heads, HEAD).transpose(1, 0, 2) * (HEAD ** (-0.5) / LN2)
-    q = q.reshape(heads * tokens, HEAD)
-    high = lax.reduce_precision(q, 8, 7)
-    q = jnp.concatenate([high, q - high], axis=1).astype(jnp.bfloat16)
+def attend(own, q, conv_in, conv_gate, conv_taps, sb_bias, nz, nt):
+    tokens = conv_in.shape[0]
+    heads = q.shape[0] // tokens
     order = jnp.arange(KEYS)
     tri = (order[:, None] > order[None, :]).astype(jnp.bfloat16)
-    cols = w_out.shape[0] // 4
-    w_rows = w_out.reshape(4, cols, 16).transpose(0, 2, 1).reshape(64, cols)
-    own = jnp.concatenate([kv, w_rows], axis=0)
     vmem = pl.BlockSpec(memory_space=pltpu.VMEM)
     out_cols = nz * 128 // nt
     wide = pltpu.VMEM((heads * tokens, 2 * HEAD), jnp.float32)
@@ -344,16 +421,6 @@
     )(sb_bias / LN2, q, own, conv_in, conv_gate, conv_taps, tri)
 
 
-def copy_for_each(value, axis):
-    copies = jnp.broadcast_to(value, (lax.axis_size(axis), *value.shape))
-    return lax.all_to_all(copies, axis, split_axis=0, concat_axis=0, tiled=True)
-
-
-def collect(value, axis):
-    parts = copy_for_each(value, axis)
-    return jnp.moveaxis(parts, 0, 1).reshape(value.shape[0], -1)
-
-
 def local(
     stream,
     norm_gain,
@@ -368,20 +435,10 @@
     w_out_conv,
 ):
     nz, nt = lax.axis_size(SP[0]), lax.axis_size("tp")
-    ins = (w_key, w_value, w_query, w_conv_in, w_conv_gate)
-    weights = gather(jnp.concatenate(ins, axis=1), nz, 0)
-    piece_f = collect(stream, "tp").astype(jnp.float32)
-    scaled = (piece_f * norm_gain[None, :]).astype(jnp.bfloat16)
-    row_scale = lax.rsqrt(jnp.sum(piece_f * piece_f, axis=1) / piece_f.shape[1] + EPS)[:, None]
-    sums = jnp.dot(scaled, weights, preferred_element_type=jnp.float32)
-    mine = (sums * row_scale).astype(jnp.bfloat16)
-    ends, at = [], w_key.shape[1]
-    for w in ins[1:-1]:
-        at += w.shape[1]
-        ends.append(at)
-    kv, query, conv_in, conv_gate = jnp.split(mine, ends, axis=1)
+    rows = jnp.concatenate([w_key, w_value, w_query, w_conv_in, w_conv_gate], axis=1)
     w_out = jnp.concatenate([w_out_attn, w_out_conv], axis=0)
-    return attend(query, kv, w_out, conv_in, conv_gate, conv_taps, sb_bias, nz, nt)
+    own, q, conv_in, conv_gate = project(rows, stream, norm_gain, w_out, nz, nt)
+    return attend(own, q, conv_in, conv_gate, conv_taps, sb_bias, nz, nt)
 
 
 def solution(mesh):

time: 124 us -> 104 us (0.84)
  Pallas kernels: 103 us -> 96.5 us
  starting transfers between devices: 5 us -> 0 us
  local copies, waits for them, and re-layouts: 7.75 us -> 4.29 us
  matrix products: 2.78 us -> 0 us
    pallas_call x1, Pallas kernels: 49.2 us -> 44 us  [project(): pl.pallas_call(functools.partial(project_kernel, nz, nt), name='project',...]
    all_to_all x1 -> x0, starting transfers between devices: 5 us -> none  [copy_for_each(): return lax.all_to_all(copies, axis, split_axis=0, concat_axis=0, tiled=True)]
    dot_general x1 -> x0, matrix products: 2.78 us -> none  [local(): sums = jnp.dot(scaled, weights, preferred_element_type=jnp.float32)]
    unnamed x5 -> x18, local copies, waits for them, and re-layouts: 3.84 us -> 2.28 us
    pallas_call x1, Pallas kernels: 53.9 us -> 52.4 us  [attend(): pl.pallas_call(functools.partial(attend_kernel, nz, nt), name='attend', o...]
    concatenate x2 -> x0, other arithmetic: 1.38 us -> none  [the longest x1 0.77 us: attend(): q = jnp.concatenate([high, q - high], axis=1).astype(jnp.bfloat16)]
    reshape x0 -> x1, local copies, waits for them, and re-layouts: none -> 1.33 us  [project(): norm_gain.reshape(nt, -1)]
  transfers between devices with their start and end apart: 1 -> 0, of which waited for: 0 -> 0; matrix products, arithmetic and copies ran while one was open for 3% -> 0% of each run, Pallas kernels for 40% -> 0%
where the time goes in v3:
time: 104 us
  Pallas kernels  96.5 us (93%)
  local copies, waits for them, and re-layouts  4.29 us (4%)
  other arithmetic  2.45 us (2%)
    pallas_call x1, Pallas kernels, attend(): pl.pallas_call(functools.partial(attend_kernel, nz, nt), name='attend', o...  52.4 us
    pallas_call x1, Pallas kernels, project(): pl.pallas_call(functools.partial(project_kernel, nz, nt), name='project',...  44 us
    unnamed x18, local copies, waits for them, and re-layouts  2.28 us

profile of v3, /device:TPU:1, one launch (start us, length us, event | category | flops | bytes accessed | tf_op | source)
XLA Modules:
  0.0 103.9 jit_solution(1418702970594452944)
XLA Ops:
  0.6 1.2 %broadcast_multiply_fusion.bias_ref = f32[4]{0:T(128)} fusion(f32[4]{0:T(128)} %param.19), kind=kLoop, calls=%fused_computation.4 | loop fusion | flops 4 | bytes 32 | tf_op jit(solution)/shard_map/div | solution.py:421
  1.8 0.0 copy-start.3
  1.8 0.0 copy-start.4
  1.8 1.3 %reshape.13.gain_ref = f32[4,512]{1,0:T(4,128)} reshape(f32[2048]{0:T(1024)} %param.12) | data formatting | bytes 16384 | tf_op jit(solution)/shard_map/reshape | solution.py:249
  3.1 0.0 copy-done.3
  3.1 0.0 copy-done.4
  3.1 0.0 copy-start
  3.1 0.0 copy-start.1
  3.1 0.0 copy-start.2
  3.2 0.0 copy-start.5
  3.2 0.0 copy-start.6
  3.2 0.6 copy_bitcast_fusion
  3.8 0.0 copy-done
  3.8 0.0 copy-done.1
  3.8 0.0 copy-done.2
  3.9 0.0 copy-done.5
  3.9 0.0 copy-done.6
  3.9 0.7 concatenate.6.own_ref
  4.6 0.7 fusion.tri_ref
  5.3 44.0 %project.1 = (bf16[192,128]{1,0:T(8,128)(2,1)}, bf16[512,128]{1,0:T(8,128)(2,1)}, bf16[128,256]{1,0:T(8,128)(2,1)}, bf16[128,256]{1,0:T(8,128)(2,1)}) custom-call(bf16[16,896]{1,0:T(8,128)(2,1)} %concatenate.6.own_ref, bf16[128,512]{1,0:T(8,128)(2,1)} %stream_ref.1, f32[4,512]{1,0:T(4,128)} %reshape.13.gain_ref, bf16[64,128]{1,0:T(8,128)(2,1)} %bitcast.8), custom_call_target="tpu_custom_call" | custom-call | tf_op jit(solution)/shard_map/project/pallas_call | solution.py:233
  49.3 52.4 %attend.1 = (bf16[128,512]{1,0:T(8,128)(2,1)}, f32[4,128]{1,0:T(4,128)}) custom-call(f32[4]{0:T(128)} %broadcast_multiply_fusion.bias_ref, bf16[512,128]{1,0:T(8,128)(2,1)} %get-tuple-element.6.q_ref, bf16[192,128]{1,0:T(8,128)(2,1)} %get-tuple-element.7.own_ref, bf16[128,256]{1,0:T(8,128)(2,1)} %get-tuple-element.8.conv_ref, ...), custom_call_target="tpu_custom_call" | custom-call | tf_op jit(solution)/shard_map/attend/pallas_call | solution.py:400
  101.7 0.0 copy-start.7
  101.7 1.6 %copy.18 = bf16[128,512]{1,0:T(8,128)(2,1)} copy(bf16[128,512]{1,0:T(8,128)(2,1)} %get-tuple-element.12) | data formatting | bytes 262144
  103.3 0.0 copy-done.7
  103.3 0.6 copy.19
Async XLA Ops:
  1.8 1.3 %copy-start.3 = (bf16[256,16]{0,1:T(8,128)(2,1)S(1)}, bf16[256,16]{0,1:T(8,128)(2,1)}, u32[]{:S(2)}) copy-start(bf16[256,16]{0,1:T(8,128)(2,1)} %param.21) | copy-start | bytes 24580
  1.8 1.3 %copy-start.4 = (bf16[256,16]{0,1:T(8,128)(2,1)S(1)}, bf16[256,16]{0,1:T(8,128)(2,1)}, u32[]{:S(2)}) copy-start(bf16[256,16]{0,1:T(8,128)(2,1)} %param.20) | copy-start | bytes 24580
  3.1 0.7 copy-start
  3.1 0.7 copy-start.1
  3.1 0.7 copy-start.2
  3.2 0.7 copy-start.5
  3.2 0.7 copy-start.6
  101.7 1.6 %copy-start.7 = (f32[4,128]{1,0:T(4,128)S(1)}, f32[4,128]{1,0:T(4,128)}, u32[]{:S(2)}) copy-start(f32[4,128]{1,0:T(4,128)} %get-tuple-element.13) | copy-start | bytes 6148

commit v4 on v3

--- a/solution.py
+++ b/solution.py
@@ -18,13 +18,48 @@
 MESH = pl.DeviceIdType.MESH
 
 
+PROJECT_ORDER = (
+    "x0", "z3", "z1", "z2", "f0", "p0", "x3", "x1", "z6", "z4", "x2", "z5",
+    "f3", "f1", "p3", "x6", "p1", "z7", "z8", "x4", "f2", "x5", "p2", "f6",
+    "x7", "p6", "x8", "f4", "f5", "p4", "p5", "f7", "f8", "p7", "p8",
+)
+ATTEND_ORDER = (
+    ("z1", "x0", "z2", "x1", "f0", "z3", "p0",),
+    ("x2", "f1", "z4", "p1",),
+    ("x3",),
+    ("z5", "f2", "x4", "z6", "p2",),
+    ("f3",),
+    ("x5", "p3", "z7",),
+    ("f4",),
+    ("z8", "x6", "p4", "f5",),
+    (),
+    ("x7", "p5",),
+    ("x8", "f6",),
+    ("p6",),
+    ("f7",),
+    ("f8", "p7",),
+    ("p8",),
+    (),
+)
+
+
+def order_of(nz, table):
+    if nz == 16:
+        return table
+    ups, downs, waits = nz // 2, (nz - 1) // 2, [("x0", "f0", "p0")]
+    for n in range(1, ups + 1):
+        waits += [tuple(kind + str(n) for kind in "zxfp"), *[()] * (n <= downs)]
+    return waits
+
+
 class Spread:
-    def __init__(self, nz, stride, own, buf, zs, zr, xs, xr, ps, pr):
+    def __init__(self, nz, stride, far_first, own, buf, zs, zr, xs, xr, ps, pr):
         self.nz, self.own, self.buf = nz, own, buf
         self.zs, self.zr, self.xs, self.xr, self.ps, self.pr = zs, zr, xs, xr, ps, pr
         self.z, self.x, self.c = (lax.axis_index(a) for a in SP)
         self.ups, self.downs = nz // 2, (nz - 1) // 2
         self.stride = min(stride, self.ups)
+        self.reach = [*range(1, self.stride + 1)][:: -1 if far_first else 1]
         self.x_up, self.x_down = ({"sp_1": lax.rem(self.x + d, 4)} for d in (1, 3))
         self.partner = {"sp_2": 1 - self.c}
         on_z = [self.z_peer(up, r) for r in range(1, self.stride + 1) for up in (True, False)]
@@ -46,7 +81,7 @@
         return n if up else self.ups + n
 
     def pass_on(self, up, n, src):
-        for r in range(self.stride, 0, -1):
+        for r in self.reach:
             k, slot = self.index(up, n + r), self.slot(up, n)
             sems = self.zs.at[k], self.zr.at[k]
             go = lambda r=r, sems=sems: remote(src, slot, *sems, self.z_peer(up, r)).start()
@@ -110,6 +145,12 @@
             self.across(up, n, 1 - self.c).wait_recv()
 
         work(True) if first else self.each(n, work)
+
+    def run(self, waits):
+        steps = {"z": self.step_z, "x": self.step_x, "f": self.step_far, "p": self.step_across}
+        for one in waits:
+            n = int(one[1:])
+            steps[one[0]](n, *([] if n else [True]))
 
     def finish(self):
         for k in range(self.nz):
@@ -150,10 +191,10 @@
 
 
 def project_kernel(
-    nz, nt, own_ref, stream_ref, gain_ref, out_rows_ref, kv_ref, q_ref, conv_ref, gate_ref,
+    nz, nt, own_ref, stream_ref, gain_ref, attn_ref, convw_ref, kv_ref, q_ref, conv_ref, gate_ref,
     buf, heard, scaled, acc, zs, zr, xs, xr, ps, pr, ys, yr,
 ):
-    net = Spread(nz, 4, own_ref, buf, zs, zr, xs, xr, ps, pr)
+    net = Spread(nz, 3, True, own_ref, buf, zs, zr, xs, xr, ps, pr)
     y = lax.axis_index("tp")
     tokens = stream_ref.shape[0]
     others = [{"tp": lax.rem(y + r, nt)} for r in range(1, nt)]
@@ -176,7 +217,7 @@
         for b in range(nt):
             piece = heard[b].astype(jnp.float32)
             squares = squares + jnp.sum(piece * piece, axis=1, keepdims=True)
-            piece = (piece * gain_ref[b : b + 1, :]).astype(jnp.bfloat16)
+            piece = (piece * gain_ref[:, b * share * 128 : (b + 1) * share * 128]).astype(jnp.bfloat16)
             for j in range(share):
                 scaled[b * share + j] = piece[:, 128 * j : 128 * (j + 1)]
         return squares
@@ -186,21 +227,18 @@
         rows = buf[at].reshape(128, acc.shape[1])
         acc[...] += jnp.dot(scaled[at], rows, preferred_element_type=jnp.float32)
 
-    near = net.stride
-    order = [0, *(q + r for q in range(0, net.ups, near) for r in range(near, 0, -1))]
+    for j in range(4):
+        source = (attn_ref, convw_ref)[j // 2]
+        kv_ref[pl.ds(tokens + 16 * j, 16), :] = source[:, 128 * (j % 2) : 128 * (j % 2 + 1)]
+
     squares = None
-    for i in range(len(order) + 6):
-        if 0 < i < len(order):
-            net.step_z(order[i])
-        if 2 <= i < len(order) + 2:
-            net.step_x(order[i - 2], i == 2)
-        if 4 <= i < len(order) + 4:
-            net.step_far(order[i - 4], i == 4)
-        if 6 <= i:
-            n = order[i - 6]
+    waits = PROJECT_ORDER if nz == 16 else [one for some in order_of(nz, None) for one in some]
+    for one in waits:
+        net.run([one])
+        if one[0] == "p":
+            n = int(one[1:])
             if n == 0:
                 squares = scale()
-            net.step_across(n, n == 0)
             take(True, n)
             if 0 < n <= net.downs:
                 take(False, n)
@@ -209,7 +247,6 @@
     wide = conv_ref.shape[1]
     heads = wide // HEAD
     kv_ref[pl.ds(0, tokens), :] = mine[:, : 2 * HEAD]
-    kv_ref[pl.ds(tokens, 64), :] = out_rows_ref[...]
     for h in range(heads):
         begin = 2 * HEAD + h * HEAD
         q = mine[:, begin : begin + HEAD].astype(jnp.float32) * (HEAD ** (-0.5) / LN2)
@@ -222,11 +259,9 @@
     net.finish()
 
 
-def project(rows, stream, norm_gain, w_out, nz, nt):
+def project(rows, stream, norm_gain, w_out_attn, w_out_conv, nz, nt):
     tokens = stream.shape[0]
     wide = (rows.shape[1] - 2 * HEAD) // 3
-    cols = w_out.shape[0] // 4
-    out_rows = w_out.reshape(4, cols, 16).transpose(0, 2, 1).reshape(64, cols)
     vmem = pl.BlockSpec(memory_space=pltpu.VMEM)
     dma = pltpu.SemaphoreType.DMA
     shapes = [(tokens + 64, 2 * HEAD), (wide // HEAD * tokens, 2 * HEAD), (tokens, wide), (tokens, wide)]
@@ -234,7 +269,7 @@
         functools.partial(project_kernel, nz, nt),
         name="project",
         out_shape=[jax.ShapeDtypeStruct(s, jnp.bfloat16) for s in shapes],
-        in_specs=[vmem] * 4,
+        in_specs=[vmem] * 5,
         out_specs=[vmem] * 4,
         scratch_shapes=[
             pltpu.VMEM((nz, 4, 2, *rows.shape), jnp.bfloat16),
@@ -246,14 +281,14 @@
             dma((nt,)),
         ],
         compiler_params=pltpu.CompilerParams(collective_id=0, has_side_effects=True),
-    )(rows, stream, norm_gain.reshape(nt, -1), out_rows)
+    )(rows, stream, norm_gain[None, :], w_out_attn.T, w_out_conv.T)
 
 
 def attend_kernel(
-    nz, nt, bias_ref, q_ref, own_ref, conv_ref, gate_ref, taps_ref, tri_ref, mixed_ref, weight_ref,
-    buf, halo, o_new, s_new, o_old, s_old, part, heard, zs, zr, xs, xr, ps, pr, hs, hr, ys, yr,
+    nz, nt, bias_ref, q_ref, own_ref, conv_ref, gate_ref, taps_ref, mixed_ref, weight_ref,
+    buf, tri, halo, o_new, s_new, o_old, s_old, part, heard, zs, zr, xs, xr, ps, pr, hs, hr, ys, yr,
 ):
-    net = Spread(nz, 2, own_ref, buf, zs, zr, xs, xr, ps, pr)
+    net = Spread(nz, 2, False, own_ref, buf, zs, zr, xs, xr, ps, pr)
     me = (net.z * 4 + net.x) * 2 + net.c
     y = lax.axis_index("tp")
     heads = bias_ref.shape[0]
@@ -269,6 +304,8 @@
     net.begin()
     tail = remote(conv_ref.at[pl.ds(rows - 16, 16), :], halo, hs, hr, ahead)
     tail.start()
+    after = lax.broadcasted_iota(jnp.int32, tri.shape, 0) > lax.broadcasted_iota(jnp.int32, tri.shape, 1)
+    tri[...] = jnp.where(after, 1.0, 0.0).astype(jnp.bfloat16)
     for ref in (o_new, s_new, o_old, s_old):
         ref[...] = jnp.zeros_like(ref)
 
@@ -279,7 +316,7 @@
             both = jnp.concatenate([kv[:, :HEAD], kv[:, :HEAD]], axis=1)
             score = lax.dot_general(q_ref[...], both, NT, preferred_element_type=jnp.float32)
             score = jnp.concatenate(
-                [score[h * rows : (h + 1) * rows] + bias_ref[h] for h in range(heads)], axis=0
+                [score[h * rows : (h + 1) * rows] + bias_ref[h] / LN2 for h in range(heads)], axis=0
             )
             if masked:
                 key_pos = i * KEYS + lax.broadcasted_iota(jnp.int32, score.shape, 1)
@@ -288,7 +325,7 @@
                 )
                 score = jnp.where(key_pos < query_pos, score, -1e30)
             fail = jnp.maximum(score, lax.log2(1.0 + jnp.exp2(jnp.minimum(score, 80.0))))
-            later = jnp.dot(fail.astype(jnp.bfloat16), tri_ref[...], preferred_element_type=jnp.float32)
+            later = jnp.dot(fail.astype(jnp.bfloat16), tri[...], preferred_element_type=jnp.float32)
             power = (score - fail) - later
             block = later[:, :1] + fail[:, :1]
             if gone is None:
@@ -312,26 +349,20 @@
         o_old[...] = o_old[...] * jnp.exp2(-gone) + out
         s_old[...] += gone
 
-    net.step_x(0, True)
-    net.step_z(1)
-    net.step_z(2)
-    net.step_far(0, True)
-    net.step_x(1)
-    net.step_z(3)
-    net.step_z(4)
-    net.step_across(0, True)
+    waits = order_of(nz, ATTEND_ORDER)
+    net.run(waits[0])
     take_new(0, True)
-    net.step_x(2)
-    net.step_far(1)
-    net.step_x(3)
+
+    def at_step(n, offset):
+        for i in range(1, net.ups + 1):
+            if 2 * i - 1 + offset < len(waits) and waits[2 * i - 1 + offset]:
+                pl.when(n == i)(functools.partial(net.run, waits[2 * i - 1 + offset]))
 
     @pl.loop(1, net.ups + 1)
     def _(n):
-        net.step_z(n + 4)
-        net.step_across(n)
+        at_step(n, 0)
         pl.when(net.z - n >= 0)(lambda: take_new(n))
-        net.step_far(n + 1)
-        net.step_x(n + 3)
+        at_step(n, 1)
         pl.when((net.z + n >= nz) & (n <= net.downs))(lambda: take_old(n))
 
     gone = s_new[...]
@@ -390,8 +421,6 @@
 def attend(own, q, conv_in, conv_gate, conv_taps, sb_bias, nz, nt):
     tokens = conv_in.shape[0]
     heads = q.shape[0] // tokens
-    order = jnp.arange(KEYS)
-    tri = (order[:, None] > order[None, :]).astype(jnp.bfloat16)
     vmem = pl.BlockSpec(memory_space=pltpu.VMEM)
     out_cols = nz * 128 // nt
     wide = pltpu.VMEM((heads * tokens, 2 * HEAD), jnp.float32)
@@ -404,10 +433,11 @@
             jax.ShapeDtypeStruct((tokens, out_cols), jnp.bfloat16),
             jax.ShapeDtypeStruct((heads, tokens), jnp.float32),
         ),
-        in_specs=[pl.BlockSpec(memory_space=pltpu.SMEM)] + [vmem] * 6,
+        in_specs=[pl.BlockSpec(memory_space=pltpu.SMEM)] + [vmem] * 5,
         out_specs=(vmem, vmem),
         scratch_shapes=[
             pltpu.VMEM((nz, 4, 2, *own.shape), jnp.bfloat16),
+            pltpu.VMEM((KEYS, KEYS), jnp.bfloat16),
             pltpu.VMEM((16, conv_in.shape[1]), jnp.bfloat16),
             *[wide] * 4,
             *[parts] * 2,
@@ -418,7 +448,7 @@
             dma((nt,)),
         ],
         compiler_params=pltpu.CompilerParams(collective_id=1, has_side_effects=True),
-    )(sb_bias / LN2, q, own, conv_in, conv_gate, conv_taps, tri)
+    )(sb_bias, q, own, conv_in, conv_gate, conv_taps)
 
 
 def local(
@@ -436,8 +466,7 @@
 ):
     nz, nt = lax.axis_size(SP[0]), lax.axis_size("tp")
     rows = jnp.concatenate([w_key, w_value, w_query, w_conv_in, w_conv_gate], axis=1)
-    w_out = jnp.concatenate([w_out_attn, w_out_conv], axis=0)
-    own, q, conv_in, conv_gate = project(rows, stream, norm_gain, w_out, nz, nt)
+    own, q, conv_in, conv_gate = project(rows, stream, norm_gain, w_out_attn, w_out_conv, nz, nt)
     return attend(own, q, conv_in, conv_gate, conv_taps, sb_bias, nz, nt)
 
 

time: 104 us -> 96.1 us (0.924)
  Pallas kernels: 96.5 us -> 90.9 us
  other arithmetic: 2.45 us -> 0 us
    pallas_call x1, Pallas kernels: 52.4 us -> 48.8 us  [attend(): pl.pallas_call(functools.partial(attend_kernel, nz, nt), name='attend', o...]
    pallas_call x1, Pallas kernels: 44 us -> 42.1 us  [project(): pl.pallas_call(functools.partial(project_kernel, nz, nt), name='project',...]
    reshape x1 -> x0, local copies, waits for them, and re-layouts: 1.33 us -> none  [project(): norm_gain.reshape(nt, -1)]
    div x1 -> x0, other arithmetic: 1.17 us -> none  [attend(): sb_bias / LN2]
    unnamed x18 -> x6, local copies, waits for them, and re-layouts: 2.28 us -> 2.83 us
where the time goes in v4:
time: 96.1 us; the launch traced here: 95.9 us
  Pallas kernels  90.9 us (95%)
  local copies, waits for them, and re-layouts  4.26 us (4%)
    pallas_call x1, Pallas kernels, attend(): pl.pallas_call(functools.partial(attend_kernel, nz, nt), name='attend', o...  48.8 us
    pallas_call x1, Pallas kernels, project(): pl.pallas_call(functools.partial(project_kernel, nz, nt), name='project',...  42.1 us
    unnamed x6, local copies, waits for them, and re-layouts  2.83 us

profile of v4, /device:TPU:1, one launch (start us, length us, event | category | flops | bytes accessed | tf_op | source)
XLA Modules:
  0.0 95.9 jit_solution(16352126709201347156)
XLA Ops:
  0.6 0.0 copy-start
  0.6 0.7 copy-done
  1.3 1.4 %concatenate.3.own_ref = bf16[16,896]{1,0:T(8,128)(2,1)} concatenate(bf16[16,64]{1,0:T(8,128)(2,1)S(1)} %copy-done, bf16[16,64]{1,0:T(8,128)(2,1)} %param.15, bf16[16,256]{1,0:T(8,128)(2,1)} %param.13, bf16[16,256]{1,0:T(8,128)(2,1)} %param.16, bf16[16,256]{1,0:T(8,128)(2,1)} %param.17), dimensions={1} | concatenate | bytes 57344 | tf_op jit(solution)/shard_map/concatenate | solution.py:468
  2.8 42.1 %project.1 = (bf16[192,128]{1,0:T(8,128)(2,1)}, bf16[512,128]{1,0:T(8,128)(2,1)}, bf16[128,256]{1,0:T(8,128)(2,1)}, bf16[128,256]{1,0:T(8,128)(2,1)}) custom-call(bf16[16,896]{1,0:T(8,128)(2,1)} %concatenate.3.own_ref, bf16[128,512]{1,0:T(8,128)(2,1)} %stream_ref.1, f32[1,2048]{1,0:T(1,128)} %bitcast.3, bf16[16,256]{1,0:T(8,128)(2,1)} %bitcast.4, ...), custom_call_target="tpu_custom_call" | custom-call | tf_op jit(solution)/shard_map/project/pallas_call | solution.py:268
  44.9 48.8 %attend.1 = (bf16[128,512]{1,0:T(8,128)(2,1)}, f32[4,128]{1,0:T(4,128)}) custom-call(f32[4]{0:T(128)} %bias_ref.1, bf16[512,128]{1,0:T(8,128)(2,1)} %get-tuple-element.6.q_ref, bf16[192,128]{1,0:T(8,128)(2,1)} %get-tuple-element.7.own_ref, bf16[128,256]{1,0:T(8,128)(2,1)} %get-tuple-element.8.conv_ref, bf16[128,256]{1,0:T(8,128)(2,1)} %get-tuple-element.9.gate_ref, ...), custom_call_target="tpu_custom_call" | custom-call | tf_op jit(solution)/shard_map/attend/pallas_call | solution.py:429
  93.7 0.0 copy-start.1
  93.7 1.6 %copy.15 = bf16[128,512]{1,0:T(8,128)(2,1)} copy(bf16[128,512]{1,0:T(8,128)(2,1)} %get-tuple-element.12) | data formatting | bytes 262144
  95.3 0.0 copy-done.1
  95.3 0.6 copy.16
Async XLA Ops:
  0.6 0.7 copy-start
  93.7 1.6 %copy-start.1 = (f32[4,128]{1,0:T(4,128)S(1)}, f32[4,128]{1,0:T(4,128)}, u32[]{:S(2)}) copy-start(f32[4,128]{1,0:T(4,128)} %get-tuple-element.13) | copy-start | bytes 6148

commit v5 on v4

v5 whole, which is shorter than its diff:
```python
import functools

import jax
import jax.numpy as jnp
from jax import lax
from jax.experimental import pallas as pl
from jax.experimental.pallas import tpu as pltpu
from jax.sharding import Mesh
from jax.sharding import PartitionSpec as P

HEAD = 64
SP = ("sp_0", "sp_1", "sp_2")
KEYS = 256
EPS = 1e-06
FLOOR = 0.02
LN2 = 0.6931471805599453
NT = (((1,), (1,)), ((), ()))
MESH = pl.DeviceIdType.MESH


PROJECT_ORDER = (
    "ix0", "iz3", "iz1", "iz2", "if0", "ip0", "ix3", "ix1", "iz6", "iz4", "ix2", "iz5",
    "if3", "if1", "ip3", "ix6", "ip1", "iz7", "iz8", "wb0", "ix4", "if2", "ix5", "ip2",
    "if6", "wz1", "ix7", "ip6", "ix8", "wx0", "if4", "if5", "wz2", "wx1", "ip4", "if7",
    "ip5", "if8", "wf0", "ip7", "wz3", "ip8",
)
ATTEND_ORDER = (
    ("wx2", "wf1", "wp0", "wp1", "wz4", "wx3", "kz1", "kx0", "wf2", "wx4", "wz5", "wp2", "wf3", "kz2", "wp3", "kx1", "kf0", "wz6", "wf4", "kz3", "wx5", "kp0",),
    ("kz4", "kx2", "kf1", "wz7", "wp4", "wx6", "kp1",),
    ("kx3", "wf5",),
    ("kz5", "kx4", "kf2", "wp5", "wz8", "wx7", "kz6", "wf6", "kp2",),
    ("kf3", "wp6",),
    ("kz7", "kx5", "kf4", "kp3",),
    ("kz8", "wx8", "kp4", "wf7",),
    ("kx6", "wp7",),
    ("kx7", "kf5",),
    ("kx8", "wf8", "kp5",),
    ("kf6", "wp8",),
    ("kf7", "kp6",),
    ("kf8", "kp7",),
    ("kp8",),
    (),
    (),
)
LAST_ORDER = ()


def orders_of(nz):
    if nz == 16:
        return PROJECT_ORDER, ATTEND_ORDER, LAST_ORDER
    ups, downs = nz // 2, (nz - 1) // 2
    first = lambda s: [s + kind + "0" for kind in "xfp"]
    waits = lambda s, n: [s + kind + str(n) for kind in "zxfp"]
    rows = [*first("i"), *(one for n in range(1, ups + 1) for one in waits("i", n))]
    keys = [first("k")]
    for n in range(1, ups + 1):
        keys += [waits("k", n), *[[]] * (n <= downs)]
    last = ["wb0", *first("w"), *(one for n in range(1, ups + 1) for one in waits("w", n))]
    return rows, keys, last


class Spread:
    def __init__(self, nz, stride, far_first, own, buf, zs, zr, xs, xr, ps, pr):
        self.nz, self.own, self.buf = nz, own, buf
        self.zs, self.zr, self.xs, self.xr, self.ps, self.pr = zs, zr, xs, xr, ps, pr
        self.z, self.x, self.c = (lax.axis_index(a) for a in SP)
        self.ups, self.downs = nz // 2, (nz - 1) // 2
        self.stride = min(stride, self.ups)
        self.reach = [*range(1, self.stride + 1)][:: -1 if far_first else 1]
        self.x_up, self.x_down = ({"sp_1": lax.rem(self.x + d, 4)} for d in (1, 3))
        self.partner = {"sp_2": 1 - self.c}
        on_z = [self.z_peer(up, r) for r in range(1, self.stride + 1) for up in (True, False)]
        self.peers = (*on_z, self.x_up, self.x_down, self.partner)

    def z_peer(self, up, r):
        return {"sp_0": lax.rem(self.z + r if up else self.z - r + self.nz, self.nz)}

    def limit(self, up):
        return self.ups if up else self.downs

    def plane(self, up, n):
        return lax.rem(self.z - n + self.nz, self.nz) if up else lax.rem(self.z + n, self.nz)

    def slot(self, up, n, dx=0):
        return self.buf.at[self.plane(up, n), lax.rem(self.x + dx, 4), self.c]

    def index(self, up, n):
        return n if up else self.ups + n

    def pass_on(self, up, n, src):
        for r in self.reach:
            k, slot = self.index(up, n + r), self.slot(up, n)
            sems = self.zs.at[k], self.zr.at[k]
            go = lambda r=r, sems=sems: remote(src, slot, *sems, self.z_peer(up, r)).start()
            when(n + r <= self.limit(up), go)

    def on_z(self, up, n):
        k, slot = self.index(up, n), self.slot(up, n)
        return remote(slot, slot, self.zs.at[k], self.zr.at[k], self.z_peer(up, 1))

    def along_x(self, up, n, way, src=None):
        k, slot = self.index(up, n), self.slot(up, n)
        peer = self.x_up if way == 0 else self.x_down
        return remote(slot if src is None else src, slot, self.xs.at[k, way], self.xr.at[k, way], peer)

    def far_x(self, up, n):
        k, slot = self.index(up, n), self.slot(up, n, 3 if up else 1)
        return remote(slot, slot, self.xs.at[k, 2], self.xr.at[k, 2], self.x_up if up else self.x_down)

    def across(self, up, n, core):
        k, row = self.index(up, n), self.buf.at[self.plane(up, n), :, core]
        return remote(row, row, self.ps.at[k], self.pr.at[k], self.partner)

    def each(self, n, work):
        when(n <= self.ups, lambda: work(True))
        when(n <= self.downs, lambda: work(False))

    def begin(self):
        own = self.own
        self.pass_on(True, 0, own)
        self.pass_on(False, 0, own)
        self.along_x(True, 0, 0, own).start()
        self.along_x(True, 0, 1, own).start()
        self.buf[self.z, self.x, self.c] = own[...]

    def step_z(self, n):
        def work(up):
            self.on_z(up, n).wait_recv()
            when(n % self.stride == 0, lambda: self.pass_on(up, n, self.slot(up, n)))
            for way in (0, 1):
                self.along_x(up, n, way).start()

        self.each(n, work)

    def step_x(self, n, first=False):
        def work(up):
            for way in (0, 1):
                self.along_x(up, n, way).wait_recv()
            self.far_x(up, n).start()

        work(True) if first else self.each(n, work)

    def step_far(self, n, first=False):
        def work(up):
            self.far_x(up, n).wait_recv()
            self.across(up, n, self.c).start()

        work(True) if first else self.each(n, work)

    def step_across(self, n, first=False):
        def work(up):
            self.across(up, n, 1 - self.c).wait_recv()

        work(True) if first else self.each(n, work)

    def finish(self):
        for k in range(self.nz):
            up = k <= self.ups
            n = k if up else k - self.ups
            if k:
                self.on_z(up, n).wait_send()
            for way in (0, 1):
                self.along_x(up, n, way).wait_send()
            self.far_x(up, n).wait_send()
            self.across(up, n, self.c).wait_send()


def remote(src, dst, ssem, rsem, peer):
    return pltpu.make_async_remote_copy(
        src_ref=src, dst_ref=dst, send_sem=ssem, recv_sem=rsem, device_id=peer, device_id_type=MESH
    )


def when(cond, work):
    if isinstance(cond, bool):
        if cond:
            work()
    else:
        pl.when(cond)(work)


def run(nets, waits):
    for one in waits:
        net, kind, n = nets[one[0]], one[1], int(one[2:])
        if kind == "b":
            net.begin()
        else:
            step = {"z": net.step_z, "x": net.step_x, "f": net.step_far, "p": net.step_across}[kind]
            step(n, *([] if n else [True]))


def greet(peers):
    barrier = pltpu.get_barrier_semaphore()
    for peer in peers:
        pl.semaphore_signal(barrier, inc=1, device_id=peer, device_id_type=MESH)
    pl.semaphore_wait(barrier, len(peers))


def spread_sems(nz):
    dma = pltpu.SemaphoreType.DMA
    return [dma((nz,)), dma((nz,)), dma((nz, 3)), dma((nz, 3)), dma((nz,)), dma((nz,))]


def layer_kernel(
    nz, nt, rows_ref, stream_ref, gain_ref, attn_ref, convw_ref, taps_ref, bias_ref, mixed_ref, weight_ref,
    rows_buf, kv_buf, out_buf, own_kv, own_out, heard, scaled, acc, q_ref, conv_ref, gate_ref,
    tri, halo, o_new, s_new, o_old, s_old, part, summed, *sems,
):
    nets = {
        "i": Spread(nz, 3, True, rows_ref, rows_buf, *sems[:6]),
        "k": Spread(nz, 2, False, own_kv, kv_buf, *sems[6:12]),
        "w": Spread(nz, 1, True, own_out, out_buf, *sems[12:18]),
    }
    net = nets["i"]
    ys, yr, hs, hr, ts, tr = sems[18:]
    project_order, attend_order, last_order = orders_of(nz)
    me = (net.z * 4 + net.x) * 2 + net.c
    y = lax.axis_index("tp")
    rows = stream_ref.shape[0]
    heads = bias_ref.shape[0]
    wide = conv_ref.shape[1]
    total = nz * 8
    share = nz // nt

    def device(index):
        return {"sp_0": lax.div(index, 8), "sp_1": lax.rem(lax.div(index, 2), 4), "sp_2": lax.rem(index, 2)}

    ahead, behind = device(lax.rem(me + 1, total)), device(lax.rem(me + total - 1, total))
    others = [{"tp": lax.rem(y + r, nt)} for r in range(1, nt)]
    greet((*net.peers, ahead, behind, *others))
    net.begin()
    sent = [
        remote(stream_ref, heard.at[y], ys.at[r], yr.at[r], others[r - 1]) for r in (2, 1, 3) if r < nt
    ]
    for one in sent:
        one.start()
    heard[y] = stream_ref[...]
    acc[...] = jnp.zeros_like(acc)
    for j in range(4):
        source = (attn_ref, convw_ref)[j // 2]
        own_out[pl.ds(16 * j, 16), :] = source[:, 128 * (j % 2) : 128 * (j % 2 + 1)]
    after = lax.broadcasted_iota(jnp.int32, tri.shape, 0) > lax.broadcasted_iota(jnp.int32, tri.shape, 1)
    tri[...] = jnp.where(after, 1.0, 0.0).astype(jnp.bfloat16)
    for ref in (o_new, s_new, o_old, s_old):
        ref[...] = jnp.zeros_like(ref)

    def scale():
        for r in range(1, nt):
            slot = heard.at[lax.rem(y + nt - r, nt)]
            remote(slot, slot, ys.at[r], yr.at[r], others[r - 1]).wait_recv()
        squares = jnp.zeros((rows, 1), jnp.float32)
        for b in range(nt):
            piece = heard[b].astype(jnp.float32)
            squares = squares + jnp.sum(piece * piece, axis=1, keepdims=True)
            piece = (piece * gain_ref[:, b * share * 128 : (b + 1) * share * 128]).astype(jnp.bfloat16)
            for j in range(share):
                scaled[b * share + j] = piece[:, 128 * j : 128 * (j + 1)]
        return squares

    def take_rows(up, n):
        at = net.plane(up, n)
        acc[...] += jnp.dot(
            scaled[at], rows_buf[at].reshape(128, acc.shape[1]), preferred_element_type=jnp.float32
        )

    squares = None
    for one in project_order:
        run(nets, [one])
        if one[:2] == "ip":
            n = int(one[2:])
            if n == 0:
                squares = scale()
            take_rows(True, n)
            if 0 < n <= net.downs:
                take_rows(False, n)
    row_scale = lax.rsqrt(squares / (nz * 128) + EPS)
    mine = (acc[...] * row_scale).astype(jnp.bfloat16)
    own_kv[...] = mine[:, : 2 * HEAD]
    conv_ref[...] = mine[:, 2 * HEAD + wide : 2 * HEAD + 2 * wide]
    gate_ref[...] = mine[:, 2 * HEAD + 2 * wide :]
    for h in range(heads):
        begin = 2 * HEAD + h * HEAD
        q = mine[:, begin : begin + HEAD].astype(jnp.float32) * (HEAD ** (-0.5) / LN2)
        high = q.astype(jnp.bfloat16).astype(jnp.float32)
        q_ref[pl.ds(h * rows, rows), :] = jnp.concatenate([high, q - high], axis=1).astype(jnp.bfloat16)
    nets["k"].begin()
    tail = remote(conv_ref.at[pl.ds(rows - 16, 16), :], halo, hs, hr, ahead)
    tail.start()

    def sweep(at, masked):
        gone, sticks, values = None, [], []
        for i in (3, 2, 1, 0):
            kv = kv_buf[at, i].reshape(KEYS, 2 * HEAD)
            both = jnp.concatenate([kv[:, :HEAD], kv[:, :HEAD]], axis=1)
            score = lax.dot_general(q_ref[...], both, NT, preferred_element_type=jnp.float32)
            score = jnp.concatenate(
                [score[h * rows : (h + 1) * rows] + bias_ref[h] / LN2 for h in range(heads)], axis=0
            )
            if masked:
                key_pos = i * KEYS + lax.broadcasted_iota(jnp.int32, score.shape, 1)
                query_pos = lax.rem(me, 8) * rows + lax.rem(
                    lax.broadcasted_iota(jnp.int32, score.shape, 0), rows
                )
                score = jnp.where(key_pos < query_pos, score, -1e30)
            fail = jnp.maximum(score, lax.log2(1.0 + jnp.exp2(jnp.minimum(score, 80.0))))
            later = jnp.dot(fail.astype(jnp.bfloat16), tri[...], preferred_element_type=jnp.float32)
            power = (score - fail) - later
            block = later[:, :1] + fail[:, :1]
            if gone is None:
                gone = jnp.broadcast_to(block, (heads * rows, 2 * HEAD))
            else:
                power = power - jnp.concatenate([gone, gone], axis=1)
                gone = gone + block
            sticks.append(jnp.exp2(power).astype(jnp.bfloat16))
            values.append(kv)
        out = jnp.dot(
            jnp.concatenate(sticks, axis=1),
            jnp.concatenate(values, axis=0),
            preferred_element_type=jnp.float32,
        )
        return out, gone

    def take_new(n, masked=False):
        out, gone = sweep(net.plane(True, n), masked)
        before = s_new[...]
        o_new[...] += jnp.exp2(-before) * out
        s_new[...] = before + gone

    def take_old(n):
        out, gone = sweep(net.plane(False, n), False)
        o_old[...] = o_old[...] * jnp.exp2(-gone) + out
        s_old[...] += gone

    run(nets, attend_order[0])
    take_new(0, True)

    def at_step(n, offset):
        for i in range(1, net.ups + 1):
            at = 2 * i - 1 + offset
            if at < len(attend_order) and attend_order[at]:
                pl.when(n == i)(functools.partial(run, nets, attend_order[at]))

    @pl.loop(1, net.ups + 1)
    def _(n):
        at_step(n, 0)
        pl.when(net.z - n >= 0)(lambda: take_new(n))
        at_step(n, 1)
        pl.when((net.z + n >= nz) & (n <= net.downs))(lambda: take_old(n))

    run(nets, last_order)
    gone = s_new[...]
    out = o_new[...] + jnp.exp2(-gone) * o_old[...]
    survived = (gone + s_old[...]) * LN2
    attended = [out[h * rows : (h + 1) * rows, HEAD:] for h in range(heads)]

    tail.wait_recv()
    now = conv_ref[...].astype(jnp.float32)
    last = halo[...].astype(jnp.float32) * jnp.where(me > 0, 1.0, 0.0)
    row = lax.broadcasted_iota(jnp.int32, now.shape, 0)
    one = jnp.where(row == 0, last[15:16], pltpu.roll(now, 1, 0))
    two = jnp.where(row == 0, last[14:15], jnp.where(row == 1, last[15:16], pltpu.roll(now, 2, 0)))
    conv = taps_ref[0:1, :] * two + taps_ref[1:2, :] * one + taps_ref[2:3, :] * now
    conv = gate_ref[...].astype(jnp.float32) * conv
    act = jnp.concatenate([*attended, conv], axis=1).astype(jnp.bfloat16)

    def project(to):
        planes = pl.ds(to * share, share)
        acc = None
        for j in range(4):
            w = out_buf[planes, :, :, pl.ds(16 * j, 16), :].reshape(share * 128, 128)
            term = lax.dot_general(
                act[:, 128 * j : 128 * (j + 1)], w, NT, preferred_element_type=jnp.float32
            )
            acc = term if acc is None else acc + term
        return acc.astype(jnp.bfloat16)

    parts = []
    for r in [*range(2, nt), 1] if nt > 1 else []:
        part[r] = project(lax.rem(y + r, nt))
        parts.append(remote(part.at[r], summed.at[r], ts.at[r], tr.at[r], others[r - 1]))
        parts[-1].start()
    mixed = project(y).astype(jnp.float32)
    weight = jnp.log(jnp.maximum(1.0 - jnp.exp(-survived), FLOOR))
    diagonal = lax.broadcasted_iota(jnp.int32, (rows, rows), 0) == lax.broadcasted_iota(
        jnp.int32, (rows, rows), 1
    )
    for h in range(heads):
        weight_ref[pl.ds(h, 1), :] = jnp.sum(
            jnp.where(diagonal, weight[h * rows : (h + 1) * rows], 0.0), axis=0, keepdims=True
        )
    for one in sent:
        one.wait_send()
    tail.wait_send()
    for each in nets.values():
        each.finish()
    for one in parts:
        one.wait_recv()
    for r in range(1, nt):
        mixed = mixed + summed[r].astype(jnp.float32)
    mixed_ref[...] = mixed.astype(jnp.bfloat16)
    for one in parts:
        one.wait_send()


def layer(rows, stream, norm_gain, w_out_attn, w_out_conv, conv_taps, sb_bias, nz, nt):
    tokens = stream.shape[0]
    heads = sb_bias.shape[0]
    wide = heads * HEAD
    vmem = pl.BlockSpec(memory_space=pltpu.VMEM)
    dma = pltpu.SemaphoreType.DMA
    half = lambda *shape: pltpu.VMEM(shape, jnp.bfloat16)
    sums = pltpu.VMEM((heads * tokens, 2 * HEAD), jnp.float32)
    return pl.pallas_call(
        functools.partial(layer_kernel, nz, nt),
        name="layer",
        out_shape=(
            jax.ShapeDtypeStruct(stream.shape, jnp.bfloat16),
            jax.ShapeDtypeStruct((heads, tokens), jnp.float32),
        ),
        in_specs=[vmem] * 6 + [pl.BlockSpec(memory_space=pltpu.SMEM)],
        out_specs=(vmem, vmem),
        scratch_shapes=[
            half(nz, 4, 2, *rows.shape),
            half(nz, 4, 2, tokens, 2 * HEAD),
            half(nz, 4, 2, 64, 128),
            half(tokens, 2 * HEAD),
            half(64, 128),
            half(nt, *stream.shape),
            half(nz, tokens, 128),
            pltpu.VMEM((tokens, rows.shape[1]), jnp.float32),
            half(heads * tokens, 2 * HEAD),
            half(tokens, wide),
            half(tokens, wide),
            half(KEYS, KEYS),
            half(16, wide),
            *[sums] * 4,
            *[half(nt, *stream.shape)] * 2,
            *spread_sems(nz),
            *spread_sems(nz),
            *spread_sems(nz),
            dma((nt,)),
            dma((nt,)),
            dma,
            dma,
            dma((nt,)),
            dma((nt,)),
        ],
        compiler_params=pltpu.CompilerParams(collective_id=0, has_side_effects=True),
    )(rows, stream, norm_gain[None, :], w_out_attn.T, w_out_conv.T, conv_taps, sb_bias)


def local(
    stream,
    norm_gain,
    w_query,
    w_key,
    w_value,
    w_conv_in,
    w_conv_gate,
    conv_taps,
    sb_bias,
    w_out_attn,
    w_out_conv,
):
    nz, nt = lax.axis_size(SP[0]), lax.axis_size("tp")
    rows = jnp.concatenate([w_key, w_value, w_query, w_conv_in, w_conv_gate], axis=1)
    return layer(rows, stream, norm_gain, w_out_attn, w_out_conv, conv_taps, sb_bias, nz, nt)


def solution(mesh):
    torus = Mesh(
        mesh.devices.reshape(mesh.shape["sp"] // 8, 4, 2, mesh.shape["tp"]),
        ("sp_0", "sp_1", "sp_2", "tp"),
    )
    return jax.shard_map(
        local,
        mesh=torus,
        in_specs=(
            P(SP, "tp"),
            P(),
            P(SP, "tp"),
            P(SP, "tp"),
            P(SP, "tp"),
            P(SP, "tp"),
            P(SP, "tp"),
            P(None, "tp"),
            P("tp"),
            P("tp", SP),
            P("tp", SP),
        ),
        out_specs=(P(SP, "tp"), P("tp", SP)),
        check_vma=False,
    )
```

time: 96.1 us -> 90 us (0.937)
  Pallas kernels: 90.9 us -> 84.9 us
    pallas_call x2 -> x1, Pallas kernels: 90.9 us -> 84.9 us  [layer(): pl.pallas_call(functools.partial(layer_kernel, nz, nt), name='layer', out...]
where the time goes in v5:
time: 90 us; the launch traced here: 89.8 us
  Pallas kernels  84.9 us (94%)
  local copies, waits for them, and re-layouts  4.26 us (5%)
    pallas_call x1, Pallas kernels, layer(): pl.pallas_call(functools.partial(layer_kernel, nz, nt), name='layer', out...  84.9 us
    unnamed x6, local copies, waits for them, and re-layouts  2.83 us

profile of v5, /device:TPU:1, one launch (start us, length us, event | category | flops | bytes accessed | tf_op | source)
XLA Modules:
  0.0 89.8 jit_solution(4446934590520337262)
XLA Ops:
  0.6 0.0 copy-start
  0.6 0.7 copy-done
  1.3 1.4 %concatenate.3.rows_ref = bf16[16,896]{1,0:T(8,128)(2,1)} concatenate(bf16[16,64]{1,0:T(8,128)(2,1)S(1)} %copy-done, bf16[16,64]{1,0:T(8,128)(2,1)} %param.15, bf16[16,256]{1,0:T(8,128)(2,1)} %param.13, bf16[16,256]{1,0:T(8,128)(2,1)} %param.16, bf16[16,256]{1,0:T(8,128)(2,1)} %param.17), dimensions={1} | concatenate | bytes 57344 | tf_op jit(solution)/shard_map/concatenate | solution.py:466
  2.8 84.9 %layer.1 = (bf16[128,512]{1,0:T(8,128)(2,1)}, f32[4,128]{1,0:T(4,128)}) custom-call(bf16[16,896]{1,0:T(8,128)(2,1)} %concatenate.3.rows_ref, bf16[128,512]{1,0:T(8,128)(2,1)} %stream_ref.1, f32[1,2048]{1,0:T(1,128)} %bitcast.3, bf16[16,256]{1,0:T(8,128)(2,1)} %bitcast.4, bf16[16,256]{1,0:T(8,128)(2,1)} %bitcast.5, f32[3,256]{1,0:T(4,128)} %taps_ref.1, f32[4]{0:T(128)} %bias_ref.1), custom_call_target="tpu_custom_call" | custom-call | tf_op jit(solution)/shard_map/layer/pallas_call | solution.py:413
  87.6 0.0 copy-start.1
  87.7 1.6 %copy.15 = bf16[128,512]{1,0:T(8,128)(2,1)} copy(bf16[128,512]{1,0:T(8,128)(2,1)} %get-tuple-element.4) | data formatting | bytes 262144
  89.2 0.0 copy-done.1
  89.2 0.6 copy.16
Async XLA Ops:
  0.6 0.7 copy-start
  87.6 1.6 %copy-start.1 = (f32[4,128]{1,0:T(4,128)S(1)}, f32[4,128]{1,0:T(4,128)}, u32[]{:S(2)}) copy-start(f32[4,128]{1,0:T(4,128)} %get-tuple-element.5) | copy-start | bytes 6148

commit v6 on v5

--- a/solution.py
+++ b/solution.py
@@ -60,9 +60,9 @@
 
 
 class Spread:
-    def __init__(self, nz, stride, far_first, own, buf, zs, zr, xs, xr, ps, pr):
+    def __init__(self, nz, stride, far_first, own, buf, zs, zr, xs, xr, fr, ps, pr):
         self.nz, self.own, self.buf = nz, own, buf
-        self.zs, self.zr, self.xs, self.xr, self.ps, self.pr = zs, zr, xs, xr, ps, pr
+        self.zs, self.zr, self.xs, self.xr, self.fr, self.ps, self.pr = zs, zr, xs, xr, fr, ps, pr
         self.z, self.x, self.c = (lax.axis_index(a) for a in SP)
         self.ups, self.downs = nz // 2, (nz - 1) // 2
         self.stride = min(stride, self.ups)
@@ -90,30 +90,35 @@
     def pass_on(self, up, n, src):
         for r in self.reach:
             k, slot = self.index(up, n + r), self.slot(up, n)
-            sems = self.zs.at[k], self.zr.at[k]
-            go = lambda r=r, sems=sems: remote(src, slot, *sems, self.z_peer(up, r)).start()
-            when(n + r <= self.limit(up), go)
+            sems = self.zs, self.zr.at[k]
+            if n + r <= self.limit(up):
+                remote(src, slot, *sems, self.z_peer(up, r)).start()
 
     def on_z(self, up, n):
         k, slot = self.index(up, n), self.slot(up, n)
-        return remote(slot, slot, self.zs.at[k], self.zr.at[k], self.z_peer(up, 1))
+        return remote(slot, slot, self.zs, self.zr.at[k], self.z_peer(up, 1))
 
     def along_x(self, up, n, way, src=None):
-        k, slot = self.index(up, n), self.slot(up, n)
+        slot = self.slot(up, n)
         peer = self.x_up if way == 0 else self.x_down
-        return remote(slot if src is None else src, slot, self.xs.at[k, way], self.xr.at[k, way], peer)
+        return remote(slot if src is None else src, slot, self.xs, self.xr.at[n], peer)
 
     def far_x(self, up, n):
-        k, slot = self.index(up, n), self.slot(up, n, 3 if up else 1)
-        return remote(slot, slot, self.xs.at[k, 2], self.xr.at[k, 2], self.x_up if up else self.x_down)
-
-    def across(self, up, n, core):
-        k, row = self.index(up, n), self.buf.at[self.plane(up, n), :, core]
-        return remote(row, row, self.ps.at[k], self.pr.at[k], self.partner)
-
-    def each(self, n, work):
-        when(n <= self.ups, lambda: work(True))
-        when(n <= self.downs, lambda: work(False))
+        slot = self.slot(up, n, 3 if up else 1)
+        return remote(slot, slot, self.xs, self.fr.at[n], self.x_up if up else self.x_down)
+
+    def across(self, up, n):
+        row = self.buf.at[self.plane(up, n), :, self.c]
+        return remote(row, row, self.ps, self.pr.at[n], self.partner)
+
+    def rings(self, n):
+        return [True] * (n <= self.ups) + [False] * (0 < n <= self.downs)
+
+    def arrived(self, like, rsem):
+        remote(like, like, self.xs, rsem, self.partner).wait_recv()
+
+    def left(self, like, ssem):
+        remote(like, like, ssem, self.zr.at[0], self.partner).wait_send()
 
     def begin(self):
         own = self.own
@@ -124,59 +129,42 @@
         self.buf[self.z, self.x, self.c] = own[...]
 
     def step_z(self, n):
-        def work(up):
+        for up in self.rings(n):
             self.on_z(up, n).wait_recv()
-            when(n % self.stride == 0, lambda: self.pass_on(up, n, self.slot(up, n)))
+            if n % self.stride == 0:
+                self.pass_on(up, n, self.slot(up, n))
             for way in (0, 1):
                 self.along_x(up, n, way).start()
 
-        self.each(n, work)
-
-    def step_x(self, n, first=False):
-        def work(up):
-            for way in (0, 1):
-                self.along_x(up, n, way).wait_recv()
+    def step_x(self, n):
+        rings = self.rings(n)
+        if rings:
+            self.arrived(self.buf.at[0, pl.ds(0, 2 * len(rings)), self.c], self.xr.at[n])
+        for up in rings:
             self.far_x(up, n).start()
 
-        work(True) if first else self.each(n, work)
-
-    def step_far(self, n, first=False):
-        def work(up):
-            self.far_x(up, n).wait_recv()
-            self.across(up, n, self.c).start()
-
-        work(True) if first else self.each(n, work)
-
-    def step_across(self, n, first=False):
-        def work(up):
-            self.across(up, n, 1 - self.c).wait_recv()
-
-        work(True) if first else self.each(n, work)
+    def step_far(self, n):
+        rings = self.rings(n)
+        if rings:
+            self.arrived(self.buf.at[0, pl.ds(0, len(rings)), self.c], self.fr.at[n])
+        for up in rings:
+            self.across(up, n).start()
+
+    def step_across(self, n):
+        rings = self.rings(n)
+        if rings:
+            self.arrived(self.buf.at[pl.ds(0, len(rings)), :, 1 - self.c], self.pr.at[n])
 
     def finish(self):
-        for k in range(self.nz):
-            up = k <= self.ups
-            n = k if up else k - self.ups
-            if k:
-                self.on_z(up, n).wait_send()
-            for way in (0, 1):
-                self.along_x(up, n, way).wait_send()
-            self.far_x(up, n).wait_send()
-            self.across(up, n, self.c).wait_send()
+        self.left(self.buf.at[pl.ds(0, self.nz - 1), 0, 0], self.zs)
+        self.left(self.buf.at[:, pl.ds(0, 3), 0], self.xs)
+        self.left(self.buf.at[:, :, 0], self.ps)
 
 
 def remote(src, dst, ssem, rsem, peer):
     return pltpu.make_async_remote_copy(
         src_ref=src, dst_ref=dst, send_sem=ssem, recv_sem=rsem, device_id=peer, device_id_type=MESH
     )
-
-
-def when(cond, work):
-    if isinstance(cond, bool):
-        if cond:
-            work()
-    else:
-        pl.when(cond)(work)
 
 
 def run(nets, waits):
@@ -186,7 +174,7 @@
             net.begin()
         else:
             step = {"z": net.step_z, "x": net.step_x, "f": net.step_far, "p": net.step_across}[kind]
-            step(n, *([] if n else [True]))
+            step(n)
 
 
 def greet(peers):
@@ -197,8 +185,8 @@
 
 
 def spread_sems(nz):
-    dma = pltpu.SemaphoreType.DMA
-    return [dma((nz,)), dma((nz,)), dma((nz, 3)), dma((nz, 3)), dma((nz,)), dma((nz,))]
+    dma, steps = pltpu.SemaphoreType.DMA, nz // 2 + 1
+    return [dma, dma((nz,)), dma, dma((steps,)), dma((steps,)), dma, dma((steps,))]
 
 
 def layer_kernel(
@@ -207,12 +195,12 @@
     tri, halo, o_new, s_new, o_old, s_old, part, summed, *sems,
 ):
     nets = {
-        "i": Spread(nz, 3, True, rows_ref, rows_buf, *sems[:6]),
-        "k": Spread(nz, 2, False, own_kv, kv_buf, *sems[6:12]),
-        "w": Spread(nz, 1, True, own_out, out_buf, *sems[12:18]),
+        "i": Spread(nz, 3, True, rows_ref, rows_buf, *sems[:7]),
+        "k": Spread(nz, 2, False, own_kv, kv_buf, *sems[7:14]),
+        "w": Spread(nz, 1, True, own_out, out_buf, *sems[14:21]),
     }
     net = nets["i"]
-    ys, yr, hs, hr, ts, tr = sems[18:]
+    ys, yr, hs, hr, ts, tr = sems[21:]
     project_order, attend_order, last_order = orders_of(nz)
     me = (net.z * 4 + net.x) * 2 + net.c
     y = lax.axis_index("tp")

time: 90 us -> 86.8 us (0.964)
  Pallas kernels: 84.9 us -> 81.6 us
    pallas_call x1, Pallas kernels: 84.9 us -> 81.6 us  [layer(): pl.pallas_call(functools.partial(layer_kernel, nz, nt), name='layer', out...]
where the time goes in v6:
time: 86.8 us; the launch traced here: 86.6 us
  Pallas kernels  81.6 us (94%)
  local copies, waits for them, and re-layouts  4.26 us (5%)
    pallas_call x1, Pallas kernels, layer(): pl.pallas_call(functools.partial(layer_kernel, nz, nt), name='layer', out...  81.6 us
    unnamed x6, local copies, waits for them, and re-layouts  2.83 us

profile of v6, /device:TPU:1, one launch (start us, length us, event | category | flops | bytes accessed | tf_op | source)
XLA Modules:
  0.0 86.6 jit_solution(945347150309360031)
XLA Ops:
  0.6 0.0 copy-start
  0.6 0.7 copy-done
  1.3 1.4 %concatenate.3.rows_ref = bf16[16,896]{1,0:T(8,128)(2,1)} concatenate(bf16[16,64]{1,0:T(8,128)(2,1)S(1)} %copy-done, bf16[16,64]{1,0:T(8,128)(2,1)} %param.15, bf16[16,256]{1,0:T(8,128)(2,1)} %param.13, bf16[16,256]{1,0:T(8,128)(2,1)} %param.16, bf16[16,256]{1,0:T(8,128)(2,1)} %param.17), dimensions={1} | concatenate | bytes 57344 | tf_op jit(solution)/shard_map/concatenate | solution.py:454
  2.8 81.6 %layer.1 = (bf16[128,512]{1,0:T(8,128)(2,1)}, f32[4,128]{1,0:T(4,128)}) custom-call(bf16[16,896]{1,0:T(8,128)(2,1)} %concatenate.3.rows_ref, bf16[128,512]{1,0:T(8,128)(2,1)} %stream_ref.1, f32[1,2048]{1,0:T(1,128)} %bitcast.3, bf16[16,256]{1,0:T(8,128)(2,1)} %bitcast.4, bf16[16,256]{1,0:T(8,128)(2,1)} %bitcast.5, f32[3,256]{1,0:T(4,128)} %taps_ref.1, f32[4]{0:T(128)} %bias_ref.1), custom_call_target="tpu_custom_call" | custom-call | tf_op jit(solution)/shard_map/layer/pallas_call | solution.py:401
  84.4 0.0 copy-start.1
  84.4 1.6 %copy.15 = bf16[128,512]{1,0:T(8,128)(2,1)} copy(bf16[128,512]{1,0:T(8,128)(2,1)} %get-tuple-element.4) | data formatting | bytes 262144
  86.0 0.0 copy-done.1
  86.0 0.6 copy.16
Async XLA Ops:
  0.6 0.7 copy-start
  84.4 1.6 %copy-start.1 = (f32[4,128]{1,0:T(4,128)S(1)}, f32[4,128]{1,0:T(4,128)}, u32[]{:S(2)}) copy-start(f32[4,128]{1,0:T(4,128)} %get-tuple-element.5) | copy-start | bytes 6148
